TPU v7x, 128 devices: a whole 4x4x4 slice. The times are simulated.
128 devices in a mesh: sp: 16 (over z, x), fs: 4 (over y), tp: 2 (over core).
Axes of the slice: x: 4, y: 4, z: 4, core: 2. Of those that a mesh axis runs over, the one named last changes fastest.
Arguments:
- stream: bfloat16 [4, 16384, 2048], P('fs', 'sp', 'tp'), parts along dimension 0, may hold values from -6 to 6
- w_pool_in: bfloat16 [2048, 1024], P(None, 'tp'), may hold values from -0.125 to 0.125
- w_query: bfloat16 [2048, 1024], P(None, 'tp'), may hold values from -0.125 to 0.125
- w_forget: bfloat16 [2048, 1024], P(None, 'tp'), may hold values from -0.125 to 0.125
- w_value: bfloat16 [2048, 1024], P(None, 'tp'), may hold values from -0.125 to 0.125
- w_outgate: bfloat16 [2048, 1024], P(None, 'tp'), may hold values from -0.125 to 0.125
- pool_mix: bfloat16 [4, 256, 256], P('tp'), may hold values from -0.375 to 0.375
- pool_scale: float32 [1024], P('tp'), may hold values from 0.1 to 1.9
- lower_bound: float32 [1024], P('tp'), may hold values from 0.9 to 1
- extra_decay: float32 [16384, 8], P('sp', 'tp'), may hold values from -0.7 to 0
- rec_gain: float32 [128], replicated, may hold values from 0.1 to 1.9
- w_out_pool: bfloat16 [1024, 2048], P('tp'), may hold values from -0.125 to 0.125
- w_out_rec: bfloat16 [1024, 2048], P('tp'), may hold values from -0.125 to 0.125
- norm_gain: float32 [2048], P('tp'), may hold values from 0.1 to 1.9
- norm_bias: float32 [2048], P('tp'), may hold values from -3 to 3
Outputs:
- layer_out: bfloat16 [4, 16384, 2048], P('fs', 'sp', 'tp'), parts along dimension 0
There are 4 independent parts, one for each index of `fs`. A program takes and returns all parts, laid end to end along the dimension named above; an argument that names none is the same for every part. Nothing has to cross between parts.
All inputs are finite; a program needn't handle non-finite values.
Results may differ from a plain program's by a relative error of at most 0.0085.
Values may be sent and summed in bfloat16 or wider, within the bound.
No kernel may reach another device: no remote copies, remote signals or barrier semaphores. Data moves between devices by JAX's collectives and lax.ppermute only.
A program may use at most 128 MiB of HBM per device.

v0:
```python
import functools

import jax
import jax.numpy as jnp
from jax import lax
from jax.experimental import pallas as pl
from jax.experimental.pallas import tpu as pltpu
from jax.sharding import Mesh
from jax.sharding import PartitionSpec as P

D = 2048
DK = 128
BLOCK = 128
MID = 63
HALO = 16
GROUP_CH = 256
SP = ("sp_0", "sp_1")
ALPHA = 2.0**0.25
EPS_RMS = 1e-06
EPS_NORM = 1e-05
F32 = jnp.float32
BF16 = jnp.bfloat16
MIB = 1 << 20

TP, ROW0, EARLY = 0, 1, 2


def mm(a, b):
    return jnp.dot(a, b, preferred_element_type=F32)


def mm_t(a, b, ca, cb):
    return lax.dot_general(a, b, (((ca,), (cb,)), ((), ())), preferred_element_type=F32)


def call(body, meta, args, in_specs, out_specs, out_shape, grid, scratch=(), vmem=20, flops=0, aliases=None):
    nbytes = sum(a.size * a.dtype.itemsize for a in args)
    return pl.pallas_call(
        body,
        grid_spec=pltpu.PrefetchScalarGridSpec(
            num_scalar_prefetch=1,
            grid=grid,
            in_specs=in_specs,
            out_specs=out_specs,
            scratch_shapes=list(scratch),
        ),
        out_shape=out_shape,
        input_output_aliases=aliases or {},
        compiler_params=pltpu.CompilerParams(
            dimension_semantics=("arbitrary",) * len(grid), vmem_limit_bytes=vmem * MIB
        ),
        cost_estimate=pl.CostEstimate(flops=flops, bytes_accessed=nbytes, transcendentals=0),
    )(meta, *args)


def rows_spec(rows, cols, first=0):
    return pl.BlockSpec((rows, cols), lambda i, m: (i + first, 0))


def whole(shape):
    return pl.BlockSpec(shape, lambda i, m: (0,) * len(shape))


def own_rows(rows, cols):
    return pl.BlockSpec((rows, cols), lambda i, m: (m[TP], 0))


def other_rows(rows, cols):
    return pl.BlockSpec((rows, cols), lambda i, m: (1 - m[TP], 0))


def side(a, b):
    return jnp.concatenate([a, b], axis=1)


def stack(a, b):
    return jnp.concatenate([a, b], axis=0)


def own_cols(m, ref, cols):
    return ref[:, pl.ds(pl.multiple_of(m[TP] * cols, cols), cols)]


def tail_body(m, x, out):
    out[...] = x[...]


def gates_body(
    heads, m, xo, xp, wfo, wfp, wv_far, lb, ed, v_out, down_out, rel_out, st_out, c_out, pay_out, own_out, state, off, wv, sem
):
    i = pl.program_id(0)
    rows = xo.shape[0]
    width = heads * DK

    load = pltpu.make_async_copy(wv_far, wv, sem)

    @pl.when(i == 0)
    def _():
        load.start()
        state[...] = jnp.zeros_like(state)
        off[...] = jnp.zeros_like(off)

    features = side(xo[...], xp[...])
    f = mm(features, stack(wfo[...], wfp[...])).astype(BF16).astype(F32)

    @pl.when(i == 0)
    def _():
        load.wait()

    half = xo.shape[1]
    wv_own = wv[pl.ds(pl.multiple_of(m[TP] * half, half), half), :]
    wv_other = wv[pl.ds(pl.multiple_of((1 - m[TP]) * half, half), half), :]
    v = mm(features, stack(wv_own, wv_other)).astype(BF16)
    v_out[...] = v
    low = lb[...]
    gap = 1.0 - low
    sig = jax.nn.sigmoid(f)
    weight = gap * (1.0 - sig)
    extra = ed[...]
    extra_hi = extra.astype(BF16).astype(F32)
    extra_rows = jnp.concatenate(
        [extra_hi, extra - extra_hi, jnp.zeros_like(extra), jnp.zeros_like(extra)], axis=0
    ).astype(BF16)
    row = lax.broadcasted_iota(jnp.int32, (4 * heads, width), 0)
    head = lax.broadcasted_iota(jnp.int32, (4 * heads, width), 1) // DK
    spread = ((row == head) | (row == head + heads)).astype(F32).astype(BF16)
    log_keep = jnp.log(low + gap * sig) + mm_t(extra_rows, spread, 0, 0)
    hi = log_keep.astype(BF16)
    lo = (log_keep - hi.astype(F32)).astype(BF16)
    t_id = lax.broadcasted_iota(jnp.int32, (BLOCK, 2 * BLOCK), 0)
    s_id = lax.broadcasted_iota(jnp.int32, (BLOCK, 2 * BLOCK), 1)
    mask = (t_id >= jnp.where(s_id >= BLOCK, s_id - BLOCK, s_id)).astype(F32).astype(BF16)
    for b in range(rows // BLOCK):
        r = slice(b * BLOCK, (b + 1) * BLOCK)
        total = mm(mask, jnp.concatenate([hi[r], lo[r]], axis=0))
        middle = total[MID : MID + 1]
        end = total[BLOCK - 1 : BLOCK]
        rel = total - middle
        rel_out[r, :] = rel
        down = weight[r] * jnp.exp(-rel)
        down_out[r, :] = down.astype(BF16)
        in_weight = (down * jnp.exp(end - middle)).astype(BF16)
        e_mid, e_end = jnp.exp(middle), jnp.exp(end)
        before = off[...]
        c_out[pl.ds(i * (rows // BLOCK) + b, 1), :] = jnp.exp(middle + before)
        off[...] = before + end
        for h in range(heads):
            c = slice(h * DK, (h + 1) * DK)
            old = state[c, :]
            st_out[b * width + h * DK : b * width + (h + 1) * DK, :] = (old * e_mid[:, c]).astype(BF16)
            state[c, :] = old * e_end[:, c] + mm_t(v[r, c], in_weight[:, c], 0, 0)

    @pl.when(i == pl.num_programs(0) - 1)
    def _():
        write_payload(heads, state[...], jnp.exp(off[...]), pay_out, own_out)


def write_payload(heads, state, decay_row, pay_out, own_out):
    width = heads * DK
    decay = jnp.concatenate(
        [decay_row[:, h * DK : (h + 1) * DK] for h in range(heads)], axis=0
    )
    pack_payload(width, state, decay, pay_out)
    own_out[:width, :] = state
    own_out[width:, :] = jnp.concatenate([decay, jnp.zeros_like(decay)], axis=0)


def pack_payload(width, state, decay, pay_out):
    hi = decay.astype(BF16).astype(F32)
    pay_out[:width, :] = state.astype(BF16)
    pay_out[width:, :] = jnp.concatenate(
        [hi, decay - hi, jnp.zeros_like(hi), jnp.zeros_like(hi)], axis=0
    ).astype(BF16)


def unpack_decay(heads, width, ref):
    rows = ref[width:, :].astype(F32)
    return rows[:heads] + rows[heads : 2 * heads]


def combine_body(heads, which, m, own, *refs):
    width = heads * DK
    if which:
        pre, recv, pay_out, pre_out = refs[:4]
        own_out = refs[4] if len(refs) > 4 else None
    else:
        recv, pay_out, pre_out, own_out = refs
    early = m[EARLY + which] == 1
    d_own = own[width : width + heads, :]
    d_pre = pre[width : width + heads, :] if which else jnp.ones((heads, DK), F32)
    d_recv = unpack_decay(heads, width, recv)
    d_all = d_own * d_recv
    new_d_pre = jnp.where(early, d_recv * d_pre, d_pre)
    pre_out[width:, :] = jnp.concatenate([new_d_pre, jnp.zeros_like(d_pre)], axis=0)
    if own_out is not None:
        own_out[width:, :] = jnp.concatenate([d_all, jnp.zeros_like(d_all)], axis=0)
    states = []
    for h in range(heads):
        c = slice(h * DK, (h + 1) * DK)
        got = recv[c, :].astype(F32)
        mine = own[c, :]
        p = pre[c, :] if which else jnp.zeros((DK, DK), F32)
        pre_out[c, :] = jnp.where(early, p + d_pre[h : h + 1] * got, p)
        new = jnp.where(early, d_own[h : h + 1] * got + mine, d_recv[h : h + 1] * mine + got)
        if own_out is not None:
            own_out[c, :] = new
        states.append(new)
    pack_payload(width, jnp.concatenate(states, axis=0), d_all, pay_out)


def pool_body(m, xo, xp, to, tp, wo, wp, mix, scale, out, ext):
    i = pl.program_id(0)
    rows = xo.shape[0]

    @pl.when(i == 0)
    def _():
        ext[:HALO, :] = mm(side(to[...], tp[...]), stack(wo[...], wp[...])).astype(BF16)

    @pl.when(i > 0)
    def _():
        ext[:HALO, :] = ext[rows : rows + HALO, :]

    ext[HALO:, :] = mm(side(xo[...], xp[...]), stack(wo[...], wp[...])).astype(BF16)
    t_id = lax.broadcasted_iota(jnp.int32, (BLOCK, BLOCK + HALO), 0)
    s_id = lax.broadcasted_iota(jnp.int32, (BLOCK, BLOCK + HALO), 1)
    lag = t_id + HALO - s_id
    row_id = lax.broadcasted_iota(jnp.int32, (BLOCK, 1), 0)
    groups = mix.shape[0]
    for j in range(groups):
        window = jnp.left_shift(1, m[TP] * groups + j + 1)
        band = ((lag >= 0) & (lag < window)).astype(F32).astype(BF16)
        c = slice(j * GROUP_CH, (j + 1) * GROUP_CH)
        for b in range(rows // BLOCK):
            position = m[ROW0] + i * rows + b * BLOCK + row_id
            share = 1.0 / jnp.minimum(position + 1, window).astype(F32)
            sums = mm(band, ext[b * BLOCK : b * BLOCK + BLOCK + HALO, c])
            here = ext[b * BLOCK + HALO : b * BLOCK + BLOCK + HALO, c].astype(F32)
            diff = (sums * share - here).astype(BF16)
            out[b * BLOCK : (b + 1) * BLOCK, c] = (mm(diff, mix[j]) * scale[:, c]).astype(BF16)


def query_body(heads, m, xo, xp, wo, wp, rel, down, q_out, s_out):
    q = mm(side(xo[...], xp[...]), stack(wo[...], wp[...])).astype(BF16).astype(F32)
    up = (jax.nn.silu(q) * jnp.exp(rel[...])).astype(BF16)
    q_out[...] = up
    t_id = lax.broadcasted_iota(jnp.int32, (BLOCK, BLOCK), 0)
    s_id = lax.broadcasted_iota(jnp.int32, (BLOCK, BLOCK), 1)
    keep = t_id >= s_id
    for b in range(up.shape[0] // BLOCK):
        r = slice(b * BLOCK, (b + 1) * BLOCK)
        for h in range(heads):
            c = slice(h * DK, (h + 1) * DK)
            score = mm_t(up[r, c], down[r, c], 1, 1)
            s_out[r, c] = jnp.where(keep, score, 0.0).astype(BF16)


def gate_body(heads, m, xo, xp, wo, wp, gain, out):
    g = mm(side(xo[...], xp[...]), stack(wo[...], wp[...])).astype(BF16).astype(F32)
    out[...] = jax.nn.silu(g) * jnp.concatenate([gain[...]] * heads, axis=1)


def rec_body(heads, start, m, scores, up, v, gate, st, cfac, pre, recv, out):
    width = heads * DK
    early = m[EARLY + 3] == 1
    factor = jnp.where(early, 1.0, 0.0)
    rows = up.shape[0]
    first = start + pl.program_id(0) * (rows // BLOCK)
    for h in range(heads):
        c = slice(h * DK, (h + 1) * DK)
        coming = pre[c, :] + (pre[width + h : width + h + 1, :] * factor) * recv[c, :].astype(F32)
        for b in range(rows // BLOCK):
            r = slice(b * BLOCK, (b + 1) * BLOCK)
            base = b * width + h * DK
            scale = cfac[pl.ds(first + b, 1), :][:, c]
            full = (st[base : base + DK, :].astype(F32) + scale * coming).astype(BF16)
            raw = mm(scores[r, c], v[r, c]) + mm_t(up[r, c], full, 1, 1)
            mean = jnp.mean(raw * raw, axis=-1, keepdims=True)
            out[r, c] = (raw * lax.rsqrt(mean + EPS_RMS) * gate[r, c]).astype(BF16)


def pool_proj_body(m, x, po, pp, wo, wp, out):
    cols = out.shape[1]
    out[...] = ALPHA * x[...].astype(F32) + mm(
        side(po[...], pp[...]), stack(own_cols(m, wo, cols), own_cols(m, wp, cols))
    )


def rec_proj_body(m, base, ro, rp, wo, wp, out, stats):
    cols = out.shape[1]
    resid = base[...] + mm(side(ro[...], rp[...]), stack(own_cols(m, wo, cols), own_cols(m, wp, cols)))
    out[...] = resid
    mean = jnp.mean(resid, axis=-1, keepdims=True)
    dev = resid - mean
    spread = jnp.sum(dev * dev, axis=-1, keepdims=True)
    lane = lax.broadcasted_iota(jnp.int32, (resid.shape[0], DK), 1)
    stats[...] = jnp.where(lane == 0, mean, spread)


def norm_body(m, resid, own, other, gain, bias, out):
    a, b = own[...], other[...]
    mean_a, mean_b = a[:, 0:1], b[:, 0:1]
    mean = 0.5 * (mean_a + mean_b)
    half = 0.5 * (mean_a - mean_b)
    var = (a[:, 1:2] + b[:, 1:2]) * (1.0 / D) + half * half
    out[...] = ((resid[...] - mean) * lax.rsqrt(var + EPS_NORM) * gain[...] + bias[...]).astype(BF16)


def last_norm_body(m, resid, own, other, gain, bias, before, out):
    norm_body(m, resid, own, other, gain, bias, out)


def shape(rows, cols, dtype):
    return jax.ShapeDtypeStruct((rows, cols), dtype)


def layer(
    stream,
    w_pool_in,
    w_query,
    w_forget,
    w_value,
    w_outgate,
    pool_mix,
    pool_scale,
    lower_bound,
    extra_decay,
    rec_gain,
    w_out_pool,
    w_out_rec,
    norm_gain,
    norm_bias,
):
    xo = stream[0]
    length, half = xo.shape
    width = lower_bound.shape[0]
    heads = width // DK
    blocks = length // BLOCK
    pool_width = w_pool_in.shape[1]
    tile_gates, tile_pool, tile_query, tile_gate, tile_base = 512, 1024, 1024, 1024, 1024
    sp_n = lax.axis_size(SP)
    z, x, k = lax.axis_index("sp_0"), lax.axis_index("sp_1"), lax.axis_index("tp")
    slot = lax.iota(jnp.int32, 8)
    meta = jnp.zeros((8,), jnp.int32)
    for at, value in enumerate((k, lax.axis_index(SP) * length, x % 2, x // 2, z % 2, z // 2)):
        meta = jnp.where(slot == at, value, meta)
    xo, meta = lax.optimization_barrier((xo, meta))
    tail = call(
        tail_body,
        meta,
        (pltpu.with_memory_space_constraint(xo, pltpu.HBM),),
        [rows_spec(HALO, half, length // HALO - 1)],
        whole((HALO, half)),
        shape(HALO, half, BF16),
        (1,),
        vmem=4,
        flops=2 * length * D * width,
    )
    swap = [(0, 1), (1, 0)]
    pairs = [(0, 1), (1, 0), (2, 3), (3, 2)]
    mirror = [(0, 3), (3, 0), (1, 2), (2, 1)]

    xp = lax.ppermute(xo, "tp", swap)
    tail_o = lax.ppermute(tail, SP, [(i, i + 1) for i in range(sp_n - 1)])
    tail_p = lax.ppermute(tail_o, "tp", swap)

    full_flops = 2 * length * D * width
    halves = lambda rows: [rows_spec(rows, half), rows_spec(rows, half)]
    full_w = lambda cols: [own_rows(half, cols), other_rows(half, cols)]
    state_rows = blocks * width
    v, down, rel, st, cfac, pay, own = call(
        functools.partial(gates_body, heads),
        meta,
        (
            xo,
            xp,
            w_forget,
            w_forget,
            pltpu.with_memory_space_constraint(w_value, pltpu.HBM),
            lower_bound.reshape(1, width),
            extra_decay.T,
        ),
        halves(tile_gates)
        + full_w(width)
        + [
            pl.BlockSpec(memory_space=pl.ANY),
            whole((1, width)),
            pl.BlockSpec((heads, tile_gates), lambda i, m: (0, i)),
        ],
        [
            rows_spec(tile_gates, width),
            rows_spec(tile_gates, width),
            rows_spec(tile_gates, width),
            rows_spec(tile_gates // BLOCK * width, DK),
            whole((blocks, width)),
            whole((width + 16, DK)),
            whole((width + 8, DK)),
        ],
        [
            shape(length, width, BF16),
            shape(length, width, BF16),
            shape(length, width, F32),
            shape(state_rows, DK, BF16),
            shape(blocks, width, F32),
            shape(width + 16, DK, BF16),
            shape(width + 8, DK, F32),
        ],
        (length // tile_gates,),
        scratch=[
            pltpu.VMEM((width, DK), F32),
            pltpu.VMEM((1, width), F32),
            pltpu.VMEM((D, width), BF16),
            pltpu.SemaphoreType.DMA,
        ],
        vmem=24,
        flops=2 * full_flops,
    )

    def combine(which, *args):
        return call(
            functools.partial(combine_body, heads, which),
            meta,
            args,
            [whole((width + 8, DK))] * (len(args) - 1) + [whole((width + 16, DK))],
            [whole((width + 16, DK))] + [whole((width + 8, DK))] * (2 - which // 2),
            [shape(width + 16, DK, BF16)] + [shape(width + 8, DK, F32)] * (2 - which // 2),
            (1,),
            vmem=4,
            flops=width * DK * 8,
        )

    got1 = lax.ppermute(pay, "sp_1", pairs)
    xo1, _ = lax.optimization_barrier((xo, pay))
    pool_o = call(
        pool_body,
        meta,
        (xo1, xp, tail_o, tail_p, w_pool_in, w_pool_in, pool_mix, pool_scale.reshape(1, pool_width)),
        halves(tile_pool)
        + [whole((HALO, half))] * 2
        + full_w(pool_width)
        + [whole(pool_mix.shape), whole((1, pool_width))],
        rows_spec(tile_pool, pool_width),
        shape(length, pool_width, BF16),
        (length // tile_pool,),
        scratch=[pltpu.VMEM((tile_pool + HALO, pool_width), BF16)],
        flops=full_flops,
    )
    pool_p = lax.ppermute(pool_o, "tp", swap)
    got1, pool_o1 = lax.optimization_barrier((got1, pool_o))
    pay2, pre2, own2 = combine(0, own, got1)

    got2 = lax.ppermute(pay2, "sp_1", mirror)
    rel1, _ = lax.optimization_barrier((rel, pay2))
    up, scores = call(
        functools.partial(query_body, heads),
        meta,
        (xo, xp, w_query, w_query, rel1, down),
        halves(tile_query) + full_w(width) + [rows_spec(tile_query, width)] * 2,
        [rows_spec(tile_query, width)] * 2,
        [shape(length, width, BF16)] * 2,
        (length // tile_query,),
        flops=full_flops,
    )
    got2, up1 = lax.optimization_barrier((got2, up))
    pay3, pre3, own3 = combine(1, own2, pre2, got2)

    got3 = lax.ppermute(pay3, "sp_0", pairs)
    xo2, _ = lax.optimization_barrier((xo, pay3))
    gate = call(
        functools.partial(gate_body, heads),
        meta,
        (xo2, xp, w_outgate, w_outgate, rec_gain.reshape(1, DK)),
        halves(tile_gate) + full_w(width) + [whole((1, DK))],
        rows_spec(tile_gate, width),
        shape(length, width, F32),
        (length // tile_gate,),
        flops=full_flops,
    )
    got3, gate1 = lax.optimization_barrier((got3, gate))
    pay4, pre4 = combine(2, own3, pre3, got3)

    got4 = lax.ppermute(pay4, "sp_0", mirror)
    wpool_p = lax.ppermute(w_out_pool, "tp", swap)
    wrec_p = lax.ppermute(w_out_rec, "tp", swap)
    pool_o2, _ = lax.optimization_barrier((pool_o1, pay4))
    base = call(
        pool_proj_body,
        meta,
        (xo, pool_o2, pool_p, w_out_pool, wpool_p),
        [rows_spec(tile_base, half), rows_spec(tile_base, pool_width), rows_spec(tile_base, pool_width)]
        + [whole((pool_width, D))] * 2,
        rows_spec(tile_base, half),
        shape(length, half, F32),
        (length // tile_base,),
        flops=full_flops,
    )
    got4, base = lax.optimization_barrier((got4, base))

    parts = 2
    rows = length // parts
    tile = rows
    per_tile = tile // BLOCK
    per = rows // tile
    recs, others = [], []
    for part in range(parts):
        first = part * per
        rec = call(
            functools.partial(rec_body, heads, part * (blocks // parts)),
            meta,
            (
                scores,
                up1,
                v,
                gate1,
                st,
                cfac,
                pre4,
                got4,
            ),
            [rows_spec(tile, width, first)] * 4
            + [
                rows_spec(per_tile * width, DK, first),
                whole((blocks, width)),
                whole((width + 8, DK)),
                whole((width + 16, DK)),
            ],
            rows_spec(tile, width),
            shape(rows, width, BF16),
            (per,),
            flops=full_flops // 4,
        )
        recs.append(rec)
        others.append(lax.ppermute(rec, "tp", swap))
    gain, bias = norm_gain.reshape(1, half), norm_bias.reshape(1, half)
    base_specs = lambda first: (
        [rows_spec(tile, half, first), rows_spec(tile, width), rows_spec(tile, width)]
        + [whole((width, D))] * 2
    )
    row_specs = [rows_spec(tile, half), rows_spec(tile, DK)]
    row_shapes = [shape(rows, half, F32), shape(rows, DK, F32)]
    resid0, stat0 = call(
        rec_proj_body,
        meta,
        (base, recs[0], others[0], w_out_rec, wrec_p),
        base_specs(0),
        row_specs,
        row_shapes,
        (per,),
        flops=full_flops // 2,
    )
    stat0_p = lax.ppermute(stat0, "tp", swap)
    resid1, stat1 = call(
        rec_proj_body,
        meta,
        (base, recs[1], others[1], w_out_rec, wrec_p),
        base_specs(per),
        row_specs,
        row_shapes,
        (per,),
        flops=full_flops // 2,
    )
    stat1_p = lax.ppermute(stat1, "tp", swap)
    resid0, _ = lax.optimization_barrier((resid0, stat1))
    fine = rows // 2
    norm_specs = [rows_spec(fine, half), rows_spec(fine, DK), rows_spec(fine, DK)] + [whole((1, half))] * 2
    out = call(
        norm_body,
        meta,
        (resid0, stat0, stat0_p, gain, bias),
        norm_specs,
        rows_spec(fine, half),
        shape(length, half, BF16),
        (rows // fine,),
        flops=full_flops // 4,
    )
    out = call(
        last_norm_body,
        meta,
        (resid1, stat1, stat1_p, gain, bias, out),
        norm_specs + [pl.BlockSpec(memory_space=pl.ANY)],
        rows_spec(fine, half, rows // fine),
        shape(length, half, BF16),
        (rows // fine,),
        flops=full_flops // 4,
        aliases={6: 0},
    )
    return out[None]


def solution(mesh):
    torus = Mesh(
        mesh.devices.reshape(4, 4, mesh.shape["fs"], mesh.shape["tp"]), ("sp_0", "sp_1", "fs", "tp")
    )
    return jax.shard_map(
        layer,
        mesh=torus,
        in_specs=(
            P("fs", SP, "tp"),
            P(None, "tp"),
            P(None, "tp"),
            P(None, "tp"),
            P(None, "tp"),
            P(None, "tp"),
            P("tp", None, None),
            P("tp"),
            P("tp"),
            P(SP, "tp"),
            P(),
            P("tp", None),
            P("tp", None),
            P("tp"),
            P("tp"),
        ),
        out_specs=P("fs", SP, "tp"),
        check_vma=False,
    )
```

profile of v0, /device:TPU:1, one launch (start us, length us, event | category | flops | bytes accessed | tf_op | source)
XLA Modules:
  0.0 63.6 jit_solution(15471127355934064847)
XLA Ops:
  0.0 0.0 copy-start.1
  0.0 0.0 copy-start
  0.0 0.0 copy-start.11
  0.0 0.0 copy-start.12
  0.1 0.0 copy-start.13
  0.1 1.4 %collective-permute-start = (bf16[1024,1024]{1,0:T(8,128)(2,1)}, bf16[1024,1024]{1,0:T(8,128)(2,1)S(1)}, u32[]{:S(2)}, u32[]{:S(2)}) collective-permute-start(bf16[1024,1024]{1,0:T(8,128)(2,1)} %bitcast.8), channel_id=1, source_target_pairs={{0,1},{1,0},{2,3},{3,2},{4,5},{5,4},{6,7},{7,6},{8,9},{9,8},{10,11... | collective-permute-start | bytes 6291464 | tf_op jit(solution)/shard_map/ppermute | solution.py:362
  1.5 0.1 collective-permute-start.8
  1.6 1.3 %shard_map.146 = bf16[16,1024]{1,0:T(8,128)(2,1)S(1)} custom-call(s32[8]{0:T(128)S(1)} %compare_select_fusion.5.m, bf16[1024,1024]{1,0:T(8,128)(2,1)} %bitcast.9), custom_call_target="tpu_custom_call" | custom-call | flops 2147483648 | bytes 2097152 | tf_op jit(solution)/shard_map/pallas_call | solution.py:38
  2.9 3.7 %collective-permute-start.2 = (bf16[16,1024]{1,0:T(8,128)(2,1)S(1)}, bf16[16,1024]{1,0:T(8,128)(2,1)S(1)}, u32[]{:S(2)}, u32[]{:S(2)}) collective-permute-start(bf16[16,1024]{1,0:T(8,128)(2,1)S(1)} %shard_map.146), channel_id=1, source_target_pairs={{0,8},{8,16},{16,24},{24,32},{32,40},{40,48},{48,56},{56,64},{64,7... | collective-permute-start | bytes 98312 | tf_op jit(solution)/shard_map/ppermute | solution.py:363
  6.6 0.9 %collective-permute-start.10 = (bf16[512,2048]{1,0:T(8,128)(2,1)S(1)}, bf16[512,2048]{1,0:T(8,128)(2,1)S(1)}, u32[]{:S(2)}, u32[]{:S(2)}) collective-permute-start(bf16[512,2048]{1,0:T(8,128)(2,1)S(1)} %copy-done.1), channel_id=1, source_target_pairs={{0,1},{1,0},{2,3},{3,2},{4,5},{5,4},{6,7},{7,6},{8,9},{9,8},{10,11... | collective-permute-start | bytes 6291464 | tf_op jit(solution)/shard_map/ppermute | solution.py:483
  7.5 0.1 collective-permute-done.2.to
  7.6 1.4 %collective-permute-start.3 = (bf16[16,1024]{1,0:T(8,128)(2,1)S(1)}, bf16[16,1024]{1,0:T(8,128)(2,1)S(1)}, u32[]{:S(2)}, u32[]{:S(2)}) collective-permute-start(bf16[16,1024]{1,0:T(8,128)(2,1)S(1)} %collective-permute-done.2.to), channel_id=1, source_target_pairs={{0,1},{1,0},{2,3},{3,2},{4,5},{5,4},{6,7},{7,6},{8,9},{9,8},{10,11... | collective-permute-start | bytes 98312 | tf_op jit(solution)/shard_map/ppermute | solution.py:364
  9.0 0.0 collective-permute-done.xp
  9.0 0.0 copy-start.2
  9.0 0.0 copy-start.6
  9.0 0.0 copy-start.9
  9.0 8.9 %shard_map.145 = (bf16[1024,512]{1,0:T(8,128)(2,1)S(1)}, bf16[1024,512]{1,0:T(8,128)(2,1)S(1)}, f32[1024,512]{1,0:T(8,128)S(1)}, bf16[4096,128]{1,0:T(8,128)(2,1...) custom-call(s32[8]{0:T(128)S(1)} %compare_select_fusion.5.m, ...), custom_call_target="tpu_custom_call" | custom-call | flops 4294967296 | bytes 10504192 | tf_op jit(solution)/shard_map/pallas_call | solution.py:38
  18.0 0.0 collective-permute-done.3.tp
  18.0 0.0 copy-start.3
  18.0 3.9 %shard_map.147.po = bf16[1024,512]{1,0:T(8,128)(2,1)S(1)} custom-call(s32[8]{0:T(128)S(1)} %compare_select_fusion.5.m, bf16[1024,1024]{1,0:T(8,128)(2,1)S(1)} %bitcast.11, bf16[1024,1024]{1,0:T(8,128)(2,1)S(1)} %collective-permute-done.xp, bf16[16,1024]{1,0:T(8,128)(2,1)S(1)} %collective-permute-done.2.to, bf16[16,1024]{1,0:T(8,128)(2,1)S(1)} %collective-permute-done.3.tp, ...), custom_call_target="tpu_custom_call" | custom-call | flops 2147483648 | bytes 8718336 | tf_op jit(solution)/shard_map/pallas_call | solution.py:38
  21.9 0.1 collective-permute-start.7
  22.0 2.1 %collective-permute-start.1 = (bf16[528,128]{1,0:T(8,128)(2,1)S(1)}, bf16[528,128]{1,0:T(8,128)(2,1)S(1)}, u32[]{:S(2)}, u32[]{:S(2)}) collective-permute-start(bf16[528,128]{1,0:T(8,128)(2,1)S(1)} %get-tuple-element.44), channel_id=1, source_target_pairs={{0,8},{8,0},{16,24},{24,16},{1,9},{9,1},{17,25},{25,17},{2,10},{10... | collective-permute-start | bytes 405512 | tf_op jit(solution)/shard_map/ppermute | solution.py:431
  24.1 3.5 %collective-permute-done.1.refs_0_ = bf16[528,128]{1,0:T(8,128)(2,1)S(1)} collective-permute-done((bf16[528,128]{1,0:T(8,128)(2,1)S(1)}, bf16[528,128]{1,0:T(8,128)(2,1)S(1)}, u32[]{:S(2)}, u32[]{:S(2)}) %collective-permute-start.1) | collective-permute-done | bytes 135200 | tf_op jit(solution)/shard_map/ppermute | solution.py:431
  27.7 0.6 shard_map.148
  28.3 2.5 %collective-permute-start.4 = (bf16[528,128]{1,0:T(8,128)(2,1)S(1)}, bf16[528,128]{1,0:T(8,128)(2,1)S(1)}, u32[]{:S(2)}, u32[]{:S(2)}) collective-permute-start(bf16[528,128]{1,0:T(8,128)(2,1)S(1)} %get-tuple-element.49), channel_id=1, source_target_pairs={{0,24},{24,0},{8,16},{16,8},{1,25},{25,1},{9,17},{17,9},{2,26},{26... | collective-permute-start | bytes 405512 | tf_op jit(solution)/shard_map/ppermute | solution.py:451
  30.8 3.9 %shard_map.149 = (bf16[1024,512]{1,0:T(8,128)(2,1)S(1)}, bf16[1024,512]{1,0:T(8,128)(2,1)S(1)}) custom-call(s32[8]{0:T(128)S(1)} %compare_select_fusion.5.m, bf16[1024,1024]{1,0:T(8,128)(2,1)S(1)} %bitcast.12, bf16[1024,1024]{1,0:T(8,128)(2,1)S(1)} %collective-permute-done.xp, bf16[2048,512]{1,0:T(8,128)(2,1)S(1)} %copy-done.3, ...), custom_call_target="tpu_custom_call" | custom-call | flops 2147483648 | bytes 11534336 | tf_op jit(solution)/shard_map/pallas_call | solution.py:38
  34.8 0.6 %shard_map.150 = (bf16[528,128]{1,0:T(8,128)(2,1)S(1)}, f32[520,128]{1,0:T(8,128)S(1)}, f32[520,128]{1,0:T(8,128)S(1)}) custom-call(s32[8]{0:T(128)S(1)} %compare_select_fusion.5.m, f32[520,128]{1,0:T(8,128)S(1)} %get-tuple-element.47.own, f32[520,128]{1,0:T(8,128)S(1)} %get-tuple-element.48.refs_0_, bf16[528,128]{1,0:T(8,128)(2,1)S(1)} %collective-permute-done.4.refs_1_), custom_call_target="tpu_custom_call" | custom-call | flops 524288 | bytes 667648 | tf_op jit(solution)/shard_map/pallas_call | solution.py:38
  35.4 2.5 %collective-permute-start.5 = (bf16[528,128]{1,0:T(8,128)(2,1)S(1)}, bf16[528,128]{1,0:T(8,128)(2,1)S(1)}, u32[]{:S(2)}, u32[]{:S(2)}) collective-permute-start(bf16[528,128]{1,0:T(8,128)(2,1)S(1)} %get-tuple-element.57), channel_id=1, source_target_pairs={{0,32},{32,0},{64,96},{96,64},{1,33},{33,1},{65,97},{97,65},{2,34}... | collective-permute-start | bytes 405512 | tf_op jit(solution)/shard_map/ppermute | solution.py:466
  37.9 3.1 %shard_map.151.gate = f32[1024,512]{1,0:T(8,128)S(1)} custom-call(s32[8]{0:T(128)S(1)} %compare_select_fusion.5.m, bf16[1024,1024]{1,0:T(8,128)(2,1)S(1)} %bitcast.13, bf16[1024,1024]{1,0:T(8,128)(2,1)S(1)} %collective-permute-done.xp, bf16[2048,512]{1,0:T(8,128)(2,1)S(1)} %copy-done.4, bf16[2048,512]{1,0:T(8,128)(2,1)S(1)} %copy-done.4, f32[1,128]{1,0:T(1,128)S(1)} %bitcast.20), custom_call_target="tpu_custom_call" | custom-call | flops 2147483648 | bytes 8389120 | tf_op jit(solution)/shard_map/pallas_call | solution.py:38
  41.0 0.6 %shard_map.152 = (bf16[528,128]{1,0:T(8,128)(2,1)S(1)}, f32[520,128]{1,0:T(8,128)S(1)}) custom-call(s32[8]{0:T(128)S(1)} %compare_select_fusion.5.m, f32[520,128]{1,0:T(8,128)S(1)} %get-tuple-element.55.own, f32[520,128]{1,0:T(8,128)S(1)} %get-tuple-element.56.refs_0_, bf16[528,128]{1,0:T(8,128)(2,1)S(1)} %collective-permute-done.5.refs_1_), custom_call_target="tpu_custom_call" | custom-call | flops 524288 | bytes 667648 | tf_op jit(solution)/shard_map/pallas_call | solution.py:38
  41.6 3.1 %collective-permute-start.6 = (bf16[528,128]{1,0:T(8,128)(2,1)S(1)}, bf16[528,128]{1,0:T(8,128)(2,1)S(1)}, u32[]{:S(2)}, u32[]{:S(2)}) collective-permute-start(bf16[528,128]{1,0:T(8,128)(2,1)S(1)} %get-tuple-element.60), channel_id=1, source_target_pairs={{0,96},{96,0},{32,64},{64,32},{1,97},{97,1},{33,65},{65,33},{2,98}... | collective-permute-start | bytes 405512 | tf_op jit(solution)/shard_map/ppermute | solution.py:481
  44.8 2.9 %shard_map.153.base = f32[1024,1024]{1,0:T(8,128)S(1)} custom-call(s32[8]{0:T(128)S(1)} %compare_select_fusion.5.m, bf16[1024,1024]{1,0:T(8,128)(2,1)S(1)} %bitcast.14, bf16[1024,512]{1,0:T(8,128)(2,1)S(1)} %shard_map.147.po, bf16[1024,512]{1,0:T(8,128)(2,1)S(1)} %collective-permute-done.7.pp, bf16[512,2048]{1,0:T(8,128)(2,1)S(1)} %copy-done.5, ...), custom_call_target="tpu_custom_call" | custom-call | flops 2147483648 | bytes 8388608 | tf_op jit(solution)/shard_map/pallas_call | solution.py:38
  47.7 0.0 collective-permute-done.6.recv
  47.7 1.4 %shard_map.156.ro = bf16[512,512]{1,0:T(8,128)(2,1)S(1)} custom-call(s32[8]{0:T(128)S(1)} %compare_select_fusion.5.m, bf16[1024,512]{1,0:T(8,128)(2,1)S(1)} %get-tuple-element.64.scores, bf16[1024,512]{1,0:T(8,128)(2,1)S(1)} %get-tuple-element.65.up, bf16[1024,512]{1,0:T(8,128)(2,1)S(1)} %get-tuple-element.66.v, f32[1024,512]{1,0:T(8,128)S(1)} %shard_map.151.gate, ...), custom_call_target="tpu_custom_call" | custom-call | flops 536870912 | bytes 6709248 | tf_op jit(solution)/shard_map/pallas_call | solution.py:38
  49.1 4.0 %collective-permute-start.12 = (bf16[512,512]{1,0:T(8,128)(2,1)S(1)}, bf16[512,512]{1,0:T(8,128)(2,1)S(1)}, u32[]{:S(2)}, u32[]{:S(2)}) collective-permute-start(bf16[512,512]{1,0:T(8,128)(2,1)S(1)} %shard_map.156.ro), channel_id=1, source_target_pairs={{0,1},{1,0},{2,3},{3,2},{4,5},{5,4},{6,7},{7,6},{8,9},{9,8},{10,11... | collective-permute-start | bytes 1572872 | tf_op jit(solution)/shard_map/ppermute | solution.py:532
  53.1 1.4 %shard_map.154.ro = bf16[512,512]{1,0:T(8,128)(2,1)S(1)} custom-call(s32[8]{0:T(128)S(1)} %compare_select_fusion.5.m, bf16[1024,512]{1,0:T(8,128)(2,1)S(1)} %get-tuple-element.64.scores, bf16[1024,512]{1,0:T(8,128)(2,1)S(1)} %get-tuple-element.65.up, bf16[1024,512]{1,0:T(8,128)(2,1)S(1)} %get-tuple-element.66.v, f32[1024,512]{1,0:T(8,128)S(1)} %shard_map.151.gate, ...), custom_call_target="tpu_custom_call" | custom-call | flops 536870912 | bytes 6709248 | tf_op jit(solution)/shard_map/pallas_call | solution.py:38
  54.5 0.1 collective-permute-start.9
  54.6 0.0 collective-permute-done.10.wp
  54.6 0.0 collective-permute-done.12.rp
  54.6 2.1 %shard_map.157 = (f32[512,1024]{1,0:T(8,128)S(1)}, f32[512,128]{1,0:T(8,128)S(1)}) custom-call(s32[8]{0:T(128)S(1)} %compare_select_fusion.5.m, f32[1024,1024]{1,0:T(8,128)S(1)} %shard_map.153.base, bf16[512,512]{1,0:T(8,128)(2,1)S(1)} %shard_map.156.ro, bf16[512,512]{1,0:T(8,128)(2,1)S(1)} %collective-permute-done.12.rp, bf16[512,2048]{1,0:T(8,128)(2,1)S(1)} %copy-done.1, ...), custom_call_target="tpu_custom_call" | custom-call | flops 1073741824 | bytes 9437184 | tf_op jit(solution)/shard_map/pallas_call | solution.py:38
  56.8 0.0 copy-start.8
  56.8 0.5 collective-permute-start.13
  57.3 0.0 collective-permute-done.9.rp
  57.3 2.2 %shard_map.155 = (f32[512,1024]{1,0:T(8,128)S(1)}, f32[512,128]{1,0:T(8,128)S(1)}) custom-call(s32[8]{0:T(128)S(1)} %compare_select_fusion.5.m, f32[1024,1024]{1,0:T(8,128)S(1)} %shard_map.153.base, bf16[512,512]{1,0:T(8,128)(2,1)S(1)} %shard_map.154.ro, bf16[512,512]{1,0:T(8,128)(2,1)S(1)} %collective-permute-done.9.rp, bf16[512,2048]{1,0:T(8,128)(2,1)S(1)} %copy-done.1, ...), custom_call_target="tpu_custom_call" | custom-call | flops 1073741824 | bytes 9437184 | tf_op jit(solution)/shard_map/pallas_call | solution.py:38
  59.5 0.1 collective-permute-start.11
  59.6 0.0 collective-permute-done.13.other
  59.6 2.0 %shard_map.158.before = bf16[1024,1024]{1,0:T(8,128)(2,1)} custom-call(s32[8]{0:T(128)S(1)} %compare_select_fusion.5.m, f32[512,1024]{1,0:T(8,128)S(1)} %get-tuple-element.75.resid, f32[512,128]{1,0:T(8,128)S(1)} %get-tuple-element.76.own, f32[512,128]{1,0:T(8,128)S(1)} %collective-permute-done.13.other, f32[1,1024]{1,0:T(1,128)S(1)} %bitcast.15, ...), custom_call_target="tpu_custom_call" | custom-call | flops 536870912 | bytes 2629632 | tf_op jit(solution)/shard_map/pallas_call | solution.py:38
  61.6 2.0 %shard_map.159 = bf16[1024,1024]{1,0:T(8,128)(2,1)} custom-call(s32[8]{0:T(128)S(1)} %compare_select_fusion.5.m, f32[512,1024]{1,0:T(8,128)S(1)} %get-tuple-element.72.resid, f32[512,128]{1,0:T(8,128)S(1)} %get-tuple-element.73.own, f32[512,128]{1,0:T(8,128)S(1)} %collective-permute-done.11.other, ...), custom_call_target="tpu_custom_call", output_to_operand_aliasing={{}: (6, {})} | custom-call | flops 536870912 | bytes 4726784 | tf_op jit(solution)/shard_map/pallas_call | solution.py:38
  (24 shorter events, 0.1 us)
Async XLA Ops:
  0.0 6.6 %copy-start.1 = (bf16[512,2048]{1,0:T(8,128)(2,1)S(1)}, bf16[512,2048]{1,0:T(8,128)(2,1)}, u32[]{:S(2)}) copy-start(bf16[512,2048]{1,0:T(8,128)(2,1)} %wo.11) | copy-start | bytes 6291460
  0.0 9.0 %copy-start = (bf16[1,1024,1024]{2,1,0:T(8,128)(2,1)S(1)}, bf16[1,1024,1024]{2,1,0:T(8,128)(2,1)}, u32[]{:S(2)}) copy-start(bf16[1,1024,1024]{2,1,0:T(8,128)(2,1)} %param.15) | copy-start | bytes 6291460
  0.0 9.0 %copy-start.11 = (bf16[2048,512]{1,0:T(8,128)(2,1)S(1)}, bf16[2048,512]{1,0:T(8,128)(2,1)}, u32[]{:S(2)}) copy-start(bf16[2048,512]{1,0:T(8,128)(2,1)} %wfp.1) | copy-start | bytes 6291460
  0.0 8.9 %copy-start.12 = (f32[1024,4]{0,1:T(4,128)S(1)}, f32[1024,4]{0,1:T(4,128)}, u32[]{:S(2)}) copy-start(f32[1024,4]{0,1:T(4,128)} %param.24) | copy-start | bytes 49156
  0.1 8.9 %copy-start.13 = (f32[512]{0:T(512)S(1)}, f32[512]{0:T(512)}, u32[]{:S(2)}) copy-start(f32[512]{0:T(512)} %param.23) | copy-start | bytes 6148
  0.1 8.9 %collective-permute-start = (bf16[1024,1024]{1,0:T(8,128)(2,1)}, bf16[1024,1024]{1,0:T(8,128)(2,1)S(1)}, u32[]{:S(2)}, u32[]{:S(2)}) collective-permute-start(bf16[1024,1024]{1,0:T(8,128)(2,1)} %bitcast.8), channel_id=1, source_target_pairs={{0,1},{1,0},{2,3},{3,2},{4,5},{5,4},{6,7},{7,6},{8,9},{9,8},{10,11... | collective-permute-start | bytes 6291464 | tf_op jit(solution)/shard_map/ppermute | solution.py:362
  1.5 43.3 %collective-permute-start.8 = (bf16[512,2048]{1,0:T(8,128)(2,1)}, bf16[512,2048]{1,0:T(8,128)(2,1)S(1)}, u32[]{:S(2)}, u32[]{:S(2)}) collective-permute-start(bf16[512,2048]{1,0:T(8,128)(2,1)} %wo.9), channel_id=1, source_target_pairs={{0,1},{1,0},{2,3},{3,2},{4,5},{5,4},{6,7},{7,6},{8,9},{9,8},{10,11... | collective-permute-start | bytes 6291464 | tf_op jit(solution)/shard_map/ppermute | solution.py:482
  2.9 4.7 %collective-permute-start.2 = (bf16[16,1024]{1,0:T(8,128)(2,1)S(1)}, bf16[16,1024]{1,0:T(8,128)(2,1)S(1)}, u32[]{:S(2)}, u32[]{:S(2)}) collective-permute-start(bf16[16,1024]{1,0:T(8,128)(2,1)S(1)} %shard_map.146), channel_id=1, source_target_pairs={{0,8},{8,16},{16,24},{24,32},{32,40},{40,48},{48,56},{56,64},{64,7... | collective-permute-start | bytes 98312 | tf_op jit(solution)/shard_map/ppermute | solution.py:363
  6.6 48.0 %collective-permute-start.10 = (bf16[512,2048]{1,0:T(8,128)(2,1)S(1)}, bf16[512,2048]{1,0:T(8,128)(2,1)S(1)}, u32[]{:S(2)}, u32[]{:S(2)}) collective-permute-start(bf16[512,2048]{1,0:T(8,128)(2,1)S(1)} %copy-done.1), channel_id=1, source_target_pairs={{0,1},{1,0},{2,3},{3,2},{4,5},{5,4},{6,7},{7,6},{8,9},{9,8},{10,11... | collective-permute-start | bytes 6291464 | tf_op jit(solution)/shard_map/ppermute | solution.py:483
  7.6 10.4 %collective-permute-start.3 = (bf16[16,1024]{1,0:T(8,128)(2,1)S(1)}, bf16[16,1024]{1,0:T(8,128)(2,1)S(1)}, u32[]{:S(2)}, u32[]{:S(2)}) collective-permute-start(bf16[16,1024]{1,0:T(8,128)(2,1)S(1)} %collective-permute-done.2.to), channel_id=1, source_target_pairs={{0,1},{1,0},{2,3},{3,2},{4,5},{5,4},{6,7},{7,6},{8,9},{9,8},{10,11... | collective-permute-start | bytes 98312 | tf_op jit(solution)/shard_map/ppermute | solution.py:364
  9.0 9.0 %copy-start.2 = (bf16[2048,512]{1,0:T(8,128)(2,1)S(1)}, bf16[2048,512]{1,0:T(8,128)(2,1)}, u32[]{:S(2)}) copy-start(bf16[2048,512]{1,0:T(8,128)(2,1)} %wp.3) | copy-start | bytes 6291460
  9.0 9.0 %copy-start.6 = (bf16[2,256,256]{2,1,0:T(8,128)(2,1)S(1)}, bf16[2,256,256]{2,1,0:T(8,128)(2,1)}, u32[]{:S(2)}) copy-start(bf16[2,256,256]{2,1,0:T(8,128)(2,1)} %mix.1) | copy-start | bytes 786436
  9.0 9.0 %copy-start.9 = (f32[512]{0:T(512)S(1)}, f32[512]{0:T(512)}, u32[]{:S(2)}) copy-start(f32[512]{0:T(512)} %param.22) | copy-start | bytes 6148
  18.0 12.8 %copy-start.3 = (bf16[2048,512]{1,0:T(8,128)(2,1)S(1)}, bf16[2048,512]{1,0:T(8,128)(2,1)}, u32[]{:S(2)}) copy-start(bf16[2048,512]{1,0:T(8,128)(2,1)} %wp.4) | copy-start | bytes 6291460
  21.9 22.9 %collective-permute-start.7 = (bf16[1024,512]{1,0:T(8,128)(2,1)S(1)}, bf16[1024,512]{1,0:T(8,128)(2,1)S(1)}, u32[]{:S(2)}, u32[]{:S(2)}) collective-permute-start(bf16[1024,512]{1,0:T(8,128)(2,1)S(1)} %shard_map.147.po), channel_id=1, source_target_pairs={{0,1},{1,0},{2,3},{3,2},{4,5},{5,4},{6,7},{7,6},{8,9},{9,8},{10,11... | collective-permute-start | bytes 3145736 | tf_op jit(solution)/shard_map/ppermute | solution.py:447
  22.0 5.7 %collective-permute-start.1 = (bf16[528,128]{1,0:T(8,128)(2,1)S(1)}, bf16[528,128]{1,0:T(8,128)(2,1)S(1)}, u32[]{:S(2)}, u32[]{:S(2)}) collective-permute-start(bf16[528,128]{1,0:T(8,128)(2,1)S(1)} %get-tuple-element.44), channel_id=1, source_target_pairs={{0,8},{8,0},{16,24},{24,16},{1,9},{9,1},{17,25},{25,17},{2,10},{10... | collective-permute-start | bytes 405512 | tf_op jit(solution)/shard_map/ppermute | solution.py:431
  28.3 6.5 %collective-permute-start.4 = (bf16[528,128]{1,0:T(8,128)(2,1)S(1)}, bf16[528,128]{1,0:T(8,128)(2,1)S(1)}, u32[]{:S(2)}, u32[]{:S(2)}) collective-permute-start(bf16[528,128]{1,0:T(8,128)(2,1)S(1)} %get-tuple-element.49), channel_id=1, source_target_pairs={{0,24},{24,0},{8,16},{16,8},{1,25},{25,1},{9,17},{17,9},{2,26},{26... | collective-permute-start | bytes 405512 | tf_op jit(solution)/shard_map/ppermute | solution.py:451
  30.8 7.1 %copy-start.4 = (bf16[2048,512]{1,0:T(8,128)(2,1)S(1)}, bf16[2048,512]{1,0:T(8,128)(2,1)}, u32[]{:S(2)}) copy-start(bf16[2048,512]{1,0:T(8,128)(2,1)} %wp.5) | copy-start | bytes 6291460
  30.8 7.1 %copy-start.10 = (f32[128]{0:T(128)S(1)}, f32[128]{0:T(128)}, u32[]{:S(2)}) copy-start(f32[128]{0:T(128)} %param.25) | copy-start | bytes 1540
  35.4 5.6 %collective-permute-start.5 = (bf16[528,128]{1,0:T(8,128)(2,1)S(1)}, bf16[528,128]{1,0:T(8,128)(2,1)S(1)}, u32[]{:S(2)}, u32[]{:S(2)}) collective-permute-start(bf16[528,128]{1,0:T(8,128)(2,1)S(1)} %get-tuple-element.57), channel_id=1, source_target_pairs={{0,32},{32,0},{64,96},{96,64},{1,33},{33,1},{65,97},{97,65},{2,34}... | collective-permute-start | bytes 405512 | tf_op jit(solution)/shard_map/ppermute | solution.py:466
  37.9 6.9 %copy-start.5 = (bf16[512,2048]{1,0:T(8,128)(2,1)S(1)}, bf16[512,2048]{1,0:T(8,128)(2,1)}, u32[]{:S(2)}) copy-start(bf16[512,2048]{1,0:T(8,128)(2,1)} %wo.9) | copy-start | bytes 6291460
  41.6 6.0 %collective-permute-start.6 = (bf16[528,128]{1,0:T(8,128)(2,1)S(1)}, bf16[528,128]{1,0:T(8,128)(2,1)S(1)}, u32[]{:S(2)}, u32[]{:S(2)}) collective-permute-start(bf16[528,128]{1,0:T(8,128)(2,1)S(1)} %get-tuple-element.60), channel_id=1, source_target_pairs={{0,96},{96,0},{32,64},{64,32},{1,97},{97,1},{33,65},{65,33},{2,98}... | collective-permute-start | bytes 405512 | tf_op jit(solution)/shard_map/ppermute | solution.py:481
  49.1 5.5 %collective-permute-start.12 = (bf16[512,512]{1,0:T(8,128)(2,1)S(1)}, bf16[512,512]{1,0:T(8,128)(2,1)S(1)}, u32[]{:S(2)}, u32[]{:S(2)}) collective-permute-start(bf16[512,512]{1,0:T(8,128)(2,1)S(1)} %shard_map.156.ro), channel_id=1, source_target_pairs={{0,1},{1,0},{2,3},{3,2},{4,5},{5,4},{6,7},{7,6},{8,9},{9,8},{10,11... | collective-permute-start | bytes 1572872 | tf_op jit(solution)/shard_map/ppermute | solution.py:532
  54.5 2.8 %collective-permute-start.9 = (bf16[512,512]{1,0:T(8,128)(2,1)S(1)}, bf16[512,512]{1,0:T(8,128)(2,1)S(1)}, u32[]{:S(2)}, u32[]{:S(2)}) collective-permute-start(bf16[512,512]{1,0:T(8,128)(2,1)S(1)} %shard_map.154.ro), channel_id=1, source_target_pairs={{0,1},{1,0},{2,3},{3,2},{4,5},{5,4},{6,7},{7,6},{8,9},{9,8},{10,11... | collective-permute-start | bytes 1572872 | tf_op jit(solution)/shard_map/ppermute | solution.py:532
  56.8 2.8 %copy-start.7 = (f32[1024]{0:T(1024)S(1)}, f32[1024]{0:T(1024)}, u32[]{:S(2)}) copy-start(f32[1024]{0:T(1024)} %param.28) | copy-start | bytes 12292
  56.8 2.8 %copy-start.8 = (f32[1024]{0:T(1024)S(1)}, f32[1024]{0:T(1024)}, u32[]{:S(2)}) copy-start(f32[1024]{0:T(1024)} %param.29) | copy-start | bytes 12292
  56.8 2.8 %collective-permute-start.13 = (f32[512,128]{1,0:T(8,128)S(1)}, f32[512,128]{1,0:T(8,128)S(1)}, u32[]{:S(2)}, u32[]{:S(2)}) collective-permute-start(f32[512,128]{1,0:T(8,128)S(1)} %get-tuple-element.76.own), channel_id=1, source_target_pairs={{0,1},{1,0},{2,3},{3,2},{4,5},{5,4},{6,7},{7,6},{8,9},{9,8},{10,11... | collective-permute-start | bytes 786440 | tf_op jit(solution)/shard_map/ppermute | solution.py:550
  59.5 2.1 %collective-permute-start.11 = (f32[512,128]{1,0:T(8,128)S(1)}, f32[512,128]{1,0:T(8,128)S(1)}, u32[]{:S(2)}, u32[]{:S(2)}) collective-permute-start(f32[512,128]{1,0:T(8,128)S(1)} %get-tuple-element.73.own), channel_id=1, source_target_pairs={{0,1},{1,0},{2,3},{3,2},{4,5},{5,4},{6,7},{7,6},{8,9},{9,8},{10,11... | collective-permute-start | bytes 786440 | tf_op jit(solution)/shard_map/ppermute | solution.py:561
where the time goes:
time: 63.8 us; the launch traced here: 63.6 us
  Pallas kernels  37 us (58%)
  starting transfers between devices  22.5 us (35%)
  waiting for transfers between devices  3.72 us (6%)
    pallas_call x15, Pallas kernels, call(): pl.pallas_call(body, grid_spec=pltpu.PrefetchScalarGridSpec(num_scalar_pr...  37 us
    ppermute x2, starting transfers between devices, layer(): others.append(lax.ppermute(rec, 'tp', swap))  4.09 us
    ppermute x1, starting transfers between devices, layer(): tail_o = lax.ppermute(tail, SP, [(i, i + 1) for i in range(sp_n - 1)])  3.68 us
    ppermute x1, waiting for transfers between devices, layer(): got1 = lax.ppermute(pay, 'sp_1', pairs)  3.55 us
    ppermute x1, starting transfers between devices, layer(): got4 = lax.ppermute(pay4, 'sp_0', mirror)  3.13 us
    ppermute x1, starting transfers between devices, layer(): got2 = lax.ppermute(pay2, 'sp_1', mirror)  2.51 us
    ppermute x1, starting transfers between devices, layer(): got3 = lax.ppermute(pay3, 'sp_0', pairs)  2.46 us
    ppermute x1, starting transfers between devices, layer(): got1 = lax.ppermute(pay, 'sp_1', pairs)  2.12 us
  transfers between devices with their start and end apart: 14, of which 2 were waited for; matrix products, arithmetic and copies ran while one was open for 0% of the time, Pallas kernels for 55%

commit v1 on v0

--- a/solution.py
+++ b/solution.py
@@ -22,8 +22,6 @@
 BF16 = jnp.bfloat16
 MIB = 1 << 20
 
-TP, ROW0, EARLY = 0, 1, 2
-
 
 def mm(a, b):
     return jnp.dot(a, b, preferred_element_type=F32)
@@ -33,40 +31,29 @@
     return lax.dot_general(a, b, (((ca,), (cb,)), ((), ())), preferred_element_type=F32)
 
 
-def call(body, meta, args, in_specs, out_specs, out_shape, grid, scratch=(), vmem=20, flops=0, aliases=None):
+def call(body, args, in_specs, out_specs, out_shape, grid, scratch=(), vmem=20, flops=0, aliases=None):
     nbytes = sum(a.size * a.dtype.itemsize for a in args)
     return pl.pallas_call(
         body,
-        grid_spec=pltpu.PrefetchScalarGridSpec(
-            num_scalar_prefetch=1,
-            grid=grid,
-            in_specs=in_specs,
-            out_specs=out_specs,
-            scratch_shapes=list(scratch),
-        ),
+        grid=grid,
+        in_specs=in_specs,
+        out_specs=out_specs,
+        scratch_shapes=list(scratch),
         out_shape=out_shape,
         input_output_aliases=aliases or {},
         compiler_params=pltpu.CompilerParams(
             dimension_semantics=("arbitrary",) * len(grid), vmem_limit_bytes=vmem * MIB
         ),
         cost_estimate=pl.CostEstimate(flops=flops, bytes_accessed=nbytes, transcendentals=0),
-    )(meta, *args)
+    )(*args)
 
 
 def rows_spec(rows, cols, first=0):
-    return pl.BlockSpec((rows, cols), lambda i, m: (i + first, 0))
+    return pl.BlockSpec((rows, cols), lambda i: (i + first, 0))
 
 
 def whole(shape):
-    return pl.BlockSpec(shape, lambda i, m: (0,) * len(shape))
-
-
-def own_rows(rows, cols):
-    return pl.BlockSpec((rows, cols), lambda i, m: (m[TP], 0))
-
-
-def other_rows(rows, cols):
-    return pl.BlockSpec((rows, cols), lambda i, m: (1 - m[TP], 0))
+    return pl.BlockSpec(shape, lambda i: (0,) * len(shape))
 
 
 def side(a, b):
@@ -77,16 +64,30 @@
     return jnp.concatenate([a, b], axis=0)
 
 
-def own_cols(m, ref, cols):
-    return ref[:, pl.ds(pl.multiple_of(m[TP] * cols, cols), cols)]
-
-
-def tail_body(m, x, out):
+def own_cols(ref, cols):
+    return ref[:, pl.ds(pl.multiple_of(lax.axis_index("tp") * cols, cols), cols)]
+
+
+def own_then_other(ref):
+    half = ref.shape[0] // 2
+    k = lax.axis_index("tp")
+    return stack(
+        ref[pl.ds(pl.multiple_of(k * half, half), half), :],
+        ref[pl.ds(pl.multiple_of((1 - k) * half, half), half), :],
+    )
+
+
+def later(which):
+    place = lax.axis_index("sp_1" if which < 2 else "sp_0")
+    return (place % 2 if which % 2 == 0 else place // 2) == 1
+
+
+def tail_body(x, out):
     out[...] = x[...]
 
 
 def gates_body(
-    heads, m, xo, xp, wfo, wfp, wv_far, lb, ed, v_out, down_out, rel_out, st_out, c_out, pay_out, own_out, state, off, wv, sem
+    heads, xo, xp, wf, wv_far, lb, ed, v_out, down_out, rel_out, st_out, c_out, pay_out, own_out, state, off, wv, sem
 ):
     i = pl.program_id(0)
     rows = xo.shape[0]
@@ -101,16 +102,13 @@
         off[...] = jnp.zeros_like(off)
 
     features = side(xo[...], xp[...])
-    f = mm(features, stack(wfo[...], wfp[...])).astype(BF16).astype(F32)
+    f = mm(features, own_then_other(wf)).astype(BF16).astype(F32)
 
     @pl.when(i == 0)
     def _():
         load.wait()
 
-    half = xo.shape[1]
-    wv_own = wv[pl.ds(pl.multiple_of(m[TP] * half, half), half), :]
-    wv_other = wv[pl.ds(pl.multiple_of((1 - m[TP]) * half, half), half), :]
-    v = mm(features, stack(wv_own, wv_other)).astype(BF16)
+    v = mm(features, own_then_other(wv)).astype(BF16)
     v_out[...] = v
     low = lb[...]
     gap = 1.0 - low
@@ -178,14 +176,14 @@
     return rows[:heads] + rows[heads : 2 * heads]
 
 
-def combine_body(heads, which, m, own, *refs):
+def combine_body(heads, which, own, *refs):
     width = heads * DK
     if which:
         pre, recv, pay_out, pre_out = refs[:4]
         own_out = refs[4] if len(refs) > 4 else None
     else:
         recv, pay_out, pre_out, own_out = refs
-    early = m[EARLY + which] == 1
+    early = later(which)
     d_own = own[width : width + heads, :]
     d_pre = pre[width : width + heads, :] if which else jnp.ones((heads, DK), F32)
     d_recv = unpack_decay(heads, width, recv)
@@ -208,30 +206,30 @@
     pack_payload(width, jnp.concatenate(states, axis=0), d_all, pay_out)
 
 
-def pool_body(m, xo, xp, to, tp, wo, wp, mix, scale, out, ext):
+def pool_body(length, xo, xp, to, tp, w, mix, scale, out, ext):
     i = pl.program_id(0)
     rows = xo.shape[0]
 
     @pl.when(i == 0)
     def _():
-        ext[:HALO, :] = mm(side(to[...], tp[...]), stack(wo[...], wp[...])).astype(BF16)
+        ext[:HALO, :] = mm(side(to[...], tp[...]), own_then_other(w)).astype(BF16)
 
     @pl.when(i > 0)
     def _():
         ext[:HALO, :] = ext[rows : rows + HALO, :]
 
-    ext[HALO:, :] = mm(side(xo[...], xp[...]), stack(wo[...], wp[...])).astype(BF16)
+    ext[HALO:, :] = mm(side(xo[...], xp[...]), own_then_other(w)).astype(BF16)
     t_id = lax.broadcasted_iota(jnp.int32, (BLOCK, BLOCK + HALO), 0)
     s_id = lax.broadcasted_iota(jnp.int32, (BLOCK, BLOCK + HALO), 1)
     lag = t_id + HALO - s_id
     row_id = lax.broadcasted_iota(jnp.int32, (BLOCK, 1), 0)
     groups = mix.shape[0]
     for j in range(groups):
-        window = jnp.left_shift(1, m[TP] * groups + j + 1)
+        window = jnp.left_shift(1, lax.axis_index("tp") * groups + j + 1)
         band = ((lag >= 0) & (lag < window)).astype(F32).astype(BF16)
         c = slice(j * GROUP_CH, (j + 1) * GROUP_CH)
         for b in range(rows // BLOCK):
-            position = m[ROW0] + i * rows + b * BLOCK + row_id
+            position = lax.axis_index(SP) * length + i * rows + b * BLOCK + row_id
             share = 1.0 / jnp.minimum(position + 1, window).astype(F32)
             sums = mm(band, ext[b * BLOCK : b * BLOCK + BLOCK + HALO, c])
             here = ext[b * BLOCK + HALO : b * BLOCK + BLOCK + HALO, c].astype(F32)
@@ -239,8 +237,8 @@
             out[b * BLOCK : (b + 1) * BLOCK, c] = (mm(diff, mix[j]) * scale[:, c]).astype(BF16)
 
 
-def query_body(heads, m, xo, xp, wo, wp, rel, down, q_out, s_out):
-    q = mm(side(xo[...], xp[...]), stack(wo[...], wp[...])).astype(BF16).astype(F32)
+def query_body(heads, xo, xp, w, rel, down, q_out, s_out):
+    q = mm(side(xo[...], xp[...]), own_then_other(w)).astype(BF16).astype(F32)
     up = (jax.nn.silu(q) * jnp.exp(rel[...])).astype(BF16)
     q_out[...] = up
     t_id = lax.broadcasted_iota(jnp.int32, (BLOCK, BLOCK), 0)
@@ -254,14 +252,14 @@
             s_out[r, c] = jnp.where(keep, score, 0.0).astype(BF16)
 
 
-def gate_body(heads, m, xo, xp, wo, wp, gain, out):
-    g = mm(side(xo[...], xp[...]), stack(wo[...], wp[...])).astype(BF16).astype(F32)
+def gate_body(heads, xo, xp, w, gain, out):
+    g = mm(side(xo[...], xp[...]), own_then_other(w)).astype(BF16).astype(F32)
     out[...] = jax.nn.silu(g) * jnp.concatenate([gain[...]] * heads, axis=1)
 
 
-def rec_body(heads, start, m, scores, up, v, gate, st, cfac, pre, recv, out):
+def rec_body(heads, start, scores, up, v, gate, st, cfac, pre, recv, out):
     width = heads * DK
-    early = m[EARLY + 3] == 1
+    early = later(3)
     factor = jnp.where(early, 1.0, 0.0)
     rows = up.shape[0]
     first = start + pl.program_id(0) * (rows // BLOCK)
@@ -278,16 +276,16 @@
             out[r, c] = (raw * lax.rsqrt(mean + EPS_RMS) * gate[r, c]).astype(BF16)
 
 
-def pool_proj_body(m, x, po, pp, wo, wp, out):
+def pool_proj_body(x, po, pp, wo, wp, out):
     cols = out.shape[1]
     out[...] = ALPHA * x[...].astype(F32) + mm(
-        side(po[...], pp[...]), stack(own_cols(m, wo, cols), own_cols(m, wp, cols))
-    )
-
-
-def rec_proj_body(m, base, ro, rp, wo, wp, out, stats):
+        side(po[...], pp[...]), stack(own_cols(wo, cols), own_cols(wp, cols))
+    )
+
+
+def rec_proj_body(base, ro, rp, wo, wp, out, stats):
     cols = out.shape[1]
-    resid = base[...] + mm(side(ro[...], rp[...]), stack(own_cols(m, wo, cols), own_cols(m, wp, cols)))
+    resid = base[...] + mm(side(ro[...], rp[...]), stack(own_cols(wo, cols), own_cols(wp, cols)))
     out[...] = resid
     mean = jnp.mean(resid, axis=-1, keepdims=True)
     dev = resid - mean
@@ -296,7 +294,7 @@
     stats[...] = jnp.where(lane == 0, mean, spread)
 
 
-def norm_body(m, resid, own, other, gain, bias, out):
+def norm_body(resid, own, other, gain, bias, out):
     a, b = own[...], other[...]
     mean_a, mean_b = a[:, 0:1], b[:, 0:1]
     mean = 0.5 * (mean_a + mean_b)
@@ -305,8 +303,8 @@
     out[...] = ((resid[...] - mean) * lax.rsqrt(var + EPS_NORM) * gain[...] + bias[...]).astype(BF16)
 
 
-def last_norm_body(m, resid, own, other, gain, bias, before, out):
-    norm_body(m, resid, own, other, gain, bias, out)
+def last_norm_body(resid, own, other, gain, bias, before, out):
+    norm_body(resid, own, other, gain, bias, out)
 
 
 def shape(rows, cols, dtype):
@@ -338,15 +336,8 @@
     pool_width = w_pool_in.shape[1]
     tile_gates, tile_pool, tile_query, tile_gate, tile_base = 512, 1024, 1024, 1024, 1024
     sp_n = lax.axis_size(SP)
-    z, x, k = lax.axis_index("sp_0"), lax.axis_index("sp_1"), lax.axis_index("tp")
-    slot = lax.iota(jnp.int32, 8)
-    meta = jnp.zeros((8,), jnp.int32)
-    for at, value in enumerate((k, lax.axis_index(SP) * length, x % 2, x // 2, z % 2, z // 2)):
-        meta = jnp.where(slot == at, value, meta)
-    xo, meta = lax.optimization_barrier((xo, meta))
     tail = call(
         tail_body,
-        meta,
         (pltpu.with_memory_space_constraint(xo, pltpu.HBM),),
         [rows_spec(HALO, half, length // HALO - 1)],
         whole((HALO, half)),
@@ -365,15 +356,13 @@
 
     full_flops = 2 * length * D * width
     halves = lambda rows: [rows_spec(rows, half), rows_spec(rows, half)]
-    full_w = lambda cols: [own_rows(half, cols), other_rows(half, cols)]
+    full_w = lambda cols: [whole((D, cols))]
     state_rows = blocks * width
     v, down, rel, st, cfac, pay, own = call(
         functools.partial(gates_body, heads),
-        meta,
         (
             xo,
             xp,
-            w_forget,
             w_forget,
             pltpu.with_memory_space_constraint(w_value, pltpu.HBM),
             lower_bound.reshape(1, width),
@@ -384,7 +373,7 @@
         + [
             pl.BlockSpec(memory_space=pl.ANY),
             whole((1, width)),
-            pl.BlockSpec((heads, tile_gates), lambda i, m: (0, i)),
+            pl.BlockSpec((heads, tile_gates), lambda i: (0, i)),
         ],
         [
             rows_spec(tile_gates, width),
@@ -418,8 +407,7 @@
     def combine(which, *args):
         return call(
             functools.partial(combine_body, heads, which),
-            meta,
-            args,
+                args,
             [whole((width + 8, DK))] * (len(args) - 1) + [whole((width + 16, DK))],
             [whole((width + 16, DK))] + [whole((width + 8, DK))] * (2 - which // 2),
             [shape(width + 16, DK, BF16)] + [shape(width + 8, DK, F32)] * (2 - which // 2),
@@ -431,9 +419,8 @@
     got1 = lax.ppermute(pay, "sp_1", pairs)
     xo1, _ = lax.optimization_barrier((xo, pay))
     pool_o = call(
-        pool_body,
-        meta,
-        (xo1, xp, tail_o, tail_p, w_pool_in, w_pool_in, pool_mix, pool_scale.reshape(1, pool_width)),
+        functools.partial(pool_body, length),
+        (xo1, xp, tail_o, tail_p, w_pool_in, pool_mix, pool_scale.reshape(1, pool_width)),
         halves(tile_pool)
         + [whole((HALO, half))] * 2
         + full_w(pool_width)
@@ -452,8 +439,7 @@
     rel1, _ = lax.optimization_barrier((rel, pay2))
     up, scores = call(
         functools.partial(query_body, heads),
-        meta,
-        (xo, xp, w_query, w_query, rel1, down),
+        (xo, xp, w_query, rel1, down),
         halves(tile_query) + full_w(width) + [rows_spec(tile_query, width)] * 2,
         [rows_spec(tile_query, width)] * 2,
         [shape(length, width, BF16)] * 2,
@@ -467,8 +453,7 @@
     xo2, _ = lax.optimization_barrier((xo, pay3))
     gate = call(
         functools.partial(gate_body, heads),
-        meta,
-        (xo2, xp, w_outgate, w_outgate, rec_gain.reshape(1, DK)),
+        (xo2, xp, w_outgate, rec_gain.reshape(1, DK)),
         halves(tile_gate) + full_w(width) + [whole((1, DK))],
         rows_spec(tile_gate, width),
         shape(length, width, F32),
@@ -484,7 +469,6 @@
     pool_o2, _ = lax.optimization_barrier((pool_o1, pay4))
     base = call(
         pool_proj_body,
-        meta,
         (xo, pool_o2, pool_p, w_out_pool, wpool_p),
         [rows_spec(tile_base, half), rows_spec(tile_base, pool_width), rows_spec(tile_base, pool_width)]
         + [whole((pool_width, D))] * 2,
@@ -505,8 +489,7 @@
         first = part * per
         rec = call(
             functools.partial(rec_body, heads, part * (blocks // parts)),
-            meta,
-            (
+                (
                 scores,
                 up1,
                 v,
@@ -539,7 +522,6 @@
     row_shapes = [shape(rows, half, F32), shape(rows, DK, F32)]
     resid0, stat0 = call(
         rec_proj_body,
-        meta,
         (base, recs[0], others[0], w_out_rec, wrec_p),
         base_specs(0),
         row_specs,
@@ -550,7 +532,6 @@
     stat0_p = lax.ppermute(stat0, "tp", swap)
     resid1, stat1 = call(
         rec_proj_body,
-        meta,
         (base, recs[1], others[1], w_out_rec, wrec_p),
         base_specs(per),
         row_specs,
@@ -564,7 +545,6 @@
     norm_specs = [rows_spec(fine, half), rows_spec(fine, DK), rows_spec(fine, DK)] + [whole((1, half))] * 2
     out = call(
         norm_body,
-        meta,
         (resid0, stat0, stat0_p, gain, bias),
         norm_specs,
         rows_spec(fine, half),
@@ -574,14 +554,13 @@
     )
     out = call(
         last_norm_body,
-        meta,
         (resid1, stat1, stat1_p, gain, bias, out),
         norm_specs + [pl.BlockSpec(memory_space=pl.ANY)],
         rows_spec(fine, half, rows // fine),
         shape(length, half, BF16),
         (rows // fine,),
         flops=full_flops // 4,
-        aliases={6: 0},
+        aliases={5: 0},
     )
     return out[None]
 

time: 63.8 us -> 57.6 us (0.903)
  Pallas kernels: 37 us -> 29.2 us
  starting transfers between devices: 22.5 us -> 23.6 us
  waiting for transfers between devices: 3.72 us -> 4.39 us
    pallas_call x15, Pallas kernels: 37 us -> 29.2 us  [call(): pl.pallas_call(body, grid=grid, in_specs=in_specs, out_specs=out_specs, s...]
  transfers between devices with their start and end apart: 14 -> 14, of which waited for: 2 -> 3; matrix products, arithmetic and copies ran while one was open for 0% -> 0% of each run, Pallas kernels for 55% -> 48%
where the time goes in v1:
time: 57.6 us; the launch traced here: 57.5 us
  Pallas kernels  29.2 us (51%)
  starting transfers between devices  23.6 us (41%)
  waiting for transfers between devices  4.39 us (8%)
    pallas_call x15, Pallas kernels, call(): pl.pallas_call(body, grid=grid, in_specs=in_specs, out_specs=out_specs, s...  29.2 us
    ppermute x2, starting transfers between devices, layer(): others.append(lax.ppermute(rec, 'tp', swap))  4.63 us
    ppermute x1, starting transfers between devices, layer(): got4 = lax.ppermute(pay4, 'sp_0', mirror)  3.65 us
    ppermute x1, waiting for transfers between devices, layer(): got1 = lax.ppermute(pay, 'sp_1', pairs)  3.55 us
    ppermute x1, starting transfers between devices, layer(): tail_o = lax.ppermute(tail, SP, [(i, i + 1) for i in range(sp_n - 1)])  3.33 us
    ppermute x1, starting transfers between devices, layer(): got3 = lax.ppermute(pay3, 'sp_0', pairs)  3 us
    ppermute x1, starting transfers between devices, layer(): got2 = lax.ppermute(pay2, 'sp_1', mirror)  2.53 us
    ppermute x1, starting transfers between devices, layer(): got1 = lax.ppermute(pay, 'sp_1', pairs)  2.12 us
  transfers between devices with their start and end apart: 14, of which 3 were waited for; matrix products, arithmetic and copies ran while one was open for 0% of the time, Pallas kernels for 48%

profile of v1, /device:TPU:1, one launch (start us, length us, event | category | flops | bytes accessed | tf_op | source)
XLA Modules:
  0.0 57.5 jit_solution(10048278818533305412)
XLA Ops:
  0.0 1.4 %collective-permute-start = (bf16[1024,1024]{1,0:T(8,128)(2,1)}, bf16[1024,1024]{1,0:T(8,128)(2,1)S(1)}, u32[]{:S(2)}, u32[]{:S(2)}) collective-permute-start(bf16[1024,1024]{1,0:T(8,128)(2,1)} %bitcast.8), channel_id=1, source_target_pairs={{0,1},{1,0},{2,3},{3,2},{4,5},{5,4},{6,7},{7,6},{8,9},{9,8},{10,11... | collective-permute-start | bytes 6291464 | tf_op jit(solution)/shard_map/ppermute | solution.py:353
  1.5 0.1 collective-permute-start.8
  1.6 1.1 %shard_map.146 = bf16[16,1024]{1,0:T(8,128)(2,1)S(1)} custom-call(bf16[1024,1024]{1,0:T(8,128)(2,1)} %bitcast.9), custom_call_target="tpu_custom_call" | custom-call | flops 2147483648 | bytes 2097152 | tf_op jit(solution)/shard_map/pallas_call | solution.py:36
  2.7 3.3 %collective-permute-start.2 = (bf16[16,1024]{1,0:T(8,128)(2,1)S(1)}, bf16[16,1024]{1,0:T(8,128)(2,1)S(1)}, u32[]{:S(2)}, u32[]{:S(2)}) collective-permute-start(bf16[16,1024]{1,0:T(8,128)(2,1)S(1)} %shard_map.146), channel_id=1, source_target_pairs={{0,8},{8,16},{16,24},{24,32},{32,40},{40,48},{48,56},{56,64},{64,7... | collective-permute-start | bytes 98312 | tf_op jit(solution)/shard_map/ppermute | solution.py:354
  6.0 0.8 %collective-permute-start.10 = (bf16[512,2048]{1,0:T(8,128)(2,1)S(1)}, bf16[512,2048]{1,0:T(8,128)(2,1)S(1)}, u32[]{:S(2)}, u32[]{:S(2)}) collective-permute-start(bf16[512,2048]{1,0:T(8,128)(2,1)S(1)} %copy-done.1), channel_id=1, source_target_pairs={{0,1},{1,0},{2,3},{3,2},{4,5},{5,4},{6,7},{7,6},{8,9},{9,8},{10,11... | collective-permute-start | bytes 6291464 | tf_op jit(solution)/shard_map/ppermute | solution.py:468
  6.8 0.2 collective-permute-done.2.to
  7.0 1.3 %collective-permute-start.3 = (bf16[16,1024]{1,0:T(8,128)(2,1)S(1)}, bf16[16,1024]{1,0:T(8,128)(2,1)S(1)}, u32[]{:S(2)}, u32[]{:S(2)}) collective-permute-start(bf16[16,1024]{1,0:T(8,128)(2,1)S(1)} %collective-permute-done.2.to), channel_id=1, source_target_pairs={{0,1},{1,0},{2,3},{3,2},{4,5},{5,4},{6,7},{7,6},{8,9},{9,8},{10,11... | collective-permute-start | bytes 98312 | tf_op jit(solution)/shard_map/ppermute | solution.py:355
  8.3 0.0 collective-permute-done.xp
  8.3 0.0 copy-start.9
  8.3 0.0 copy-start.10
  8.3 0.0 copy-start.13
  8.3 8.4 %shard_map.145 = (bf16[1024,512]{1,0:T(8,128)(2,1)S(1)}, bf16[1024,512]{1,0:T(8,128)(2,1)S(1)}, f32[1024,512]{1,0:T(8,128)S(1)}, bf16[4096,128]{1,0:T(8,128)(2,1...) custom-call(bf16[1024,1024]{1,0:T(8,128)(2,1)S(1)} %bitcast.10, ...), custom_call_target="tpu_custom_call" | custom-call | flops 4294967296 | bytes 8407040 | tf_op jit(solution)/shard_map/pallas_call | solution.py:36
  16.8 0.0 collective-permute-done.3.tp
  16.8 0.0 copy-start.2
  16.8 3.3 %shard_map.147.po = bf16[1024,512]{1,0:T(8,128)(2,1)S(1)} custom-call(bf16[1024,1024]{1,0:T(8,128)(2,1)S(1)} %bitcast.11, bf16[1024,1024]{1,0:T(8,128)(2,1)S(1)} %collective-permute-done.xp, bf16[16,1024]{1,0:T(8,128)(2,1)S(1)} %collective-permute-done.2.to, bf16[16,1024]{1,0:T(8,128)(2,1)S(1)} %collective-permute-done.3.tp, ...), custom_call_target="tpu_custom_call" | custom-call | flops 2147483648 | bytes 6621184 | tf_op jit(solution)/shard_map/pallas_call | solution.py:36
  20.1 0.1 collective-permute-start.7
  20.2 2.1 %collective-permute-start.1 = (bf16[528,128]{1,0:T(8,128)(2,1)S(1)}, bf16[528,128]{1,0:T(8,128)(2,1)S(1)}, u32[]{:S(2)}, u32[]{:S(2)}) collective-permute-start(bf16[528,128]{1,0:T(8,128)(2,1)S(1)} %get-tuple-element.40), channel_id=1, source_target_pairs={{0,8},{8,0},{16,24},{24,16},{1,9},{9,1},{17,25},{25,17},{2,10},{10... | collective-permute-start | bytes 405512 | tf_op jit(solution)/shard_map/ppermute | solution.py:419
  22.3 3.5 %collective-permute-done.1.refs_0_ = bf16[528,128]{1,0:T(8,128)(2,1)S(1)} collective-permute-done((bf16[528,128]{1,0:T(8,128)(2,1)S(1)}, bf16[528,128]{1,0:T(8,128)(2,1)S(1)}, u32[]{:S(2)}, u32[]{:S(2)}) %collective-permute-start.1) | collective-permute-done | bytes 135200 | tf_op jit(solution)/shard_map/ppermute | solution.py:419
  25.9 0.1 shard_map.148
  26.0 2.5 %collective-permute-start.4 = (bf16[528,128]{1,0:T(8,128)(2,1)S(1)}, bf16[528,128]{1,0:T(8,128)(2,1)S(1)}, u32[]{:S(2)}, u32[]{:S(2)}) collective-permute-start(bf16[528,128]{1,0:T(8,128)(2,1)S(1)} %get-tuple-element.45), channel_id=1, source_target_pairs={{0,24},{24,0},{8,16},{16,8},{1,25},{25,1},{9,17},{17,9},{2,26},{26... | collective-permute-start | bytes 405512 | tf_op jit(solution)/shard_map/ppermute | solution.py:438
  28.5 3.4 %shard_map.149 = (bf16[1024,512]{1,0:T(8,128)(2,1)S(1)}, bf16[1024,512]{1,0:T(8,128)(2,1)S(1)}) custom-call(bf16[1024,1024]{1,0:T(8,128)(2,1)S(1)} %bitcast.12, bf16[1024,1024]{1,0:T(8,128)(2,1)S(1)} %collective-permute-done.xp, bf16[2048,512]{1,0:T(8,128)(2,1)S(1)} %copy-done.2, f32[1024,512]{1,0:T(8,128)S(1)} %get-tuple-element.47.rel, ...), custom_call_target="tpu_custom_call" | custom-call | flops 2147483648 | bytes 9437184 | tf_op jit(solution)/shard_map/pallas_call | solution.py:36
  31.9 0.0 collective-permute-done.4.refs_1_
  31.9 0.1 shard_map.150
  32.0 3.0 %collective-permute-start.5 = (bf16[528,128]{1,0:T(8,128)(2,1)S(1)}, bf16[528,128]{1,0:T(8,128)(2,1)S(1)}, u32[]{:S(2)}, u32[]{:S(2)}) collective-permute-start(bf16[528,128]{1,0:T(8,128)(2,1)S(1)} %get-tuple-element.53), channel_id=1, source_target_pairs={{0,32},{32,0},{64,96},{96,64},{1,33},{33,1},{65,97},{97,65},{2,34}... | collective-permute-start | bytes 405512 | tf_op jit(solution)/shard_map/ppermute | solution.py:452
  35.0 2.6 %shard_map.151.gate = f32[1024,512]{1,0:T(8,128)S(1)} custom-call(bf16[1024,1024]{1,0:T(8,128)(2,1)S(1)} %bitcast.13, bf16[1024,1024]{1,0:T(8,128)(2,1)S(1)} %collective-permute-done.xp, bf16[2048,512]{1,0:T(8,128)(2,1)S(1)} %copy-done.3, f32[1,128]{1,0:T(1,128)S(1)} %bitcast.19), custom_call_target="tpu_custom_call" | custom-call | flops 2147483648 | bytes 6291968 | tf_op jit(solution)/shard_map/pallas_call | solution.py:36
  37.6 0.0 collective-permute-done.5.refs_1_
  37.6 0.1 shard_map.152
  37.7 3.7 %collective-permute-start.6 = (bf16[528,128]{1,0:T(8,128)(2,1)S(1)}, bf16[528,128]{1,0:T(8,128)(2,1)S(1)}, u32[]{:S(2)}, u32[]{:S(2)}) collective-permute-start(bf16[528,128]{1,0:T(8,128)(2,1)S(1)} %get-tuple-element.56), channel_id=1, source_target_pairs={{0,96},{96,0},{32,64},{64,32},{1,97},{97,1},{33,65},{65,33},{2,98}... | collective-permute-start | bytes 405512 | tf_op jit(solution)/shard_map/ppermute | solution.py:466
  41.4 0.0 collective-permute-done.8.wp
  41.4 0.0 collective-permute-done.7.pp
  41.4 2.4 %shard_map.153.base = f32[1024,1024]{1,0:T(8,128)S(1)} custom-call(bf16[1024,1024]{1,0:T(8,128)(2,1)S(1)} %bitcast.14, bf16[1024,512]{1,0:T(8,128)(2,1)S(1)} %shard_map.147.po, bf16[1024,512]{1,0:T(8,128)(2,1)S(1)} %collective-permute-done.7.pp, bf16[512,2048]{1,0:T(8,128)(2,1)S(1)} %copy-done.4, bf16[512,2048]{1,0:T(8,128)(2,1)S(1)} %collective-permute-done.8.wp), custom_call_target="tpu_custom_call" | custom-call | flops 2147483648 | bytes 8388608 | tf_op jit(solution)/shard_map/pallas_call | solution.py:36
  43.7 0.0 collective-permute-done.6.recv
  43.8 0.9 %shard_map.156.ro = bf16[512,512]{1,0:T(8,128)(2,1)S(1)} custom-call(bf16[1024,512]{1,0:T(8,128)(2,1)S(1)} %get-tuple-element.60.scores, bf16[1024,512]{1,0:T(8,128)(2,1)S(1)} %get-tuple-element.61.up, bf16[1024,512]{1,0:T(8,128)(2,1)S(1)} %get-tuple-element.62.v, f32[1024,512]{1,0:T(8,128)S(1)} %shard_map.151.gate, ...), custom_call_target="tpu_custom_call" | custom-call | flops 536870912 | bytes 6709248 | tf_op jit(solution)/shard_map/pallas_call | solution.py:36
  44.6 4.5 %collective-permute-start.12 = (bf16[512,512]{1,0:T(8,128)(2,1)S(1)}, bf16[512,512]{1,0:T(8,128)(2,1)S(1)}, u32[]{:S(2)}, u32[]{:S(2)}) collective-permute-start(bf16[512,512]{1,0:T(8,128)(2,1)S(1)} %shard_map.156.ro), channel_id=1, source_target_pairs={{0,1},{1,0},{2,3},{3,2},{4,5},{5,4},{6,7},{7,6},{8,9},{9,8},{10,11... | collective-permute-start | bytes 1572872 | tf_op jit(solution)/shard_map/ppermute | solution.py:515
  49.2 0.8 %shard_map.154.ro = bf16[512,512]{1,0:T(8,128)(2,1)S(1)} custom-call(bf16[1024,512]{1,0:T(8,128)(2,1)S(1)} %get-tuple-element.60.scores, bf16[1024,512]{1,0:T(8,128)(2,1)S(1)} %get-tuple-element.61.up, bf16[1024,512]{1,0:T(8,128)(2,1)S(1)} %get-tuple-element.62.v, f32[1024,512]{1,0:T(8,128)S(1)} %shard_map.151.gate, ...), custom_call_target="tpu_custom_call" | custom-call | flops 536870912 | bytes 6709248 | tf_op jit(solution)/shard_map/pallas_call | solution.py:36
  50.0 0.1 collective-permute-start.9
  50.1 0.0 collective-permute-done.10.wp
  50.1 0.6 collective-permute-done.12.rp
  50.7 1.6 %shard_map.157 = (f32[512,1024]{1,0:T(8,128)S(1)}, f32[512,128]{1,0:T(8,128)S(1)}) custom-call(f32[1024,1024]{1,0:T(8,128)S(1)} %shard_map.153.base, bf16[512,512]{1,0:T(8,128)(2,1)S(1)} %shard_map.156.ro, bf16[512,512]{1,0:T(8,128)(2,1)S(1)} %collective-permute-done.12.rp, bf16[512,2048]{1,0:T(8,128)(2,1)S(1)} %copy-done.1, ...), custom_call_target="tpu_custom_call" | custom-call | flops 1073741824 | bytes 9437184 | tf_op jit(solution)/shard_map/pallas_call | solution.py:36
  52.3 0.0 copy-start.6
  52.3 0.5 collective-permute-start.13
  52.7 0.0 collective-permute-done.9.rp
  52.7 1.6 %shard_map.155 = (f32[512,1024]{1,0:T(8,128)S(1)}, f32[512,128]{1,0:T(8,128)S(1)}) custom-call(f32[1024,1024]{1,0:T(8,128)S(1)} %shard_map.153.base, bf16[512,512]{1,0:T(8,128)(2,1)S(1)} %shard_map.154.ro, bf16[512,512]{1,0:T(8,128)(2,1)S(1)} %collective-permute-done.9.rp, bf16[512,2048]{1,0:T(8,128)(2,1)S(1)} %copy-done.1, ...), custom_call_target="tpu_custom_call" | custom-call | flops 1073741824 | bytes 9437184 | tf_op jit(solution)/shard_map/pallas_call | solution.py:36
  54.3 0.2 collective-permute-start.11
  54.5 0.0 collective-permute-done.13.other
  54.6 1.5 %shard_map.158.before = bf16[1024,1024]{1,0:T(8,128)(2,1)} custom-call(f32[512,1024]{1,0:T(8,128)S(1)} %get-tuple-element.71.resid, f32[512,128]{1,0:T(8,128)S(1)} %get-tuple-element.72.own, f32[512,128]{1,0:T(8,128)S(1)} %collective-permute-done.13.other, f32[1,1024]{1,0:T(1,128)S(1)} %bitcast.15, f32[1,1024]{1,0:T(1,128)S(1)} %bitcast.17), custom_call_target="tpu_custom_call" | custom-call | flops 536870912 | bytes 2629632 | tf_op jit(solution)/shard_map/pallas_call | solution.py:36
  56.0 0.0 collective-permute-done.11.other
  56.0 1.4 %shard_map.159 = bf16[1024,1024]{1,0:T(8,128)(2,1)} custom-call(f32[512,1024]{1,0:T(8,128)S(1)} %get-tuple-element.68.resid, f32[512,128]{1,0:T(8,128)S(1)} %get-tuple-element.69.own, f32[512,128]{1,0:T(8,128)S(1)} %collective-permute-done.11.other, f32[1,1024]{1,0:T(1,128)S(1)} %bitcast.16, f32[1,1024]{1,0:T(1,128)S(1)} %bitcast.18, ...), custom_call_target="tpu_custom_call", output_to_operand_aliasing={{}: (5, {})} | custom-call | flops 536870912 | bytes 4726784 | tf_op jit(solution)/shard_map/pallas_call | solution.py:36
  (23 shorter events, 0.0 us)
Async XLA Ops:
  0.0 6.0 %copy-start.1 = (bf16[512,2048]{1,0:T(8,128)(2,1)S(1)}, bf16[512,2048]{1,0:T(8,128)(2,1)}, u32[]{:S(2)}) copy-start(bf16[512,2048]{1,0:T(8,128)(2,1)} %wo.5) | copy-start | bytes 6291460
  0.0 8.3 %copy-start = (bf16[1,1024,1024]{2,1,0:T(8,128)(2,1)S(1)}, bf16[1,1024,1024]{2,1,0:T(8,128)(2,1)}, u32[]{:S(2)}) copy-start(bf16[1,1024,1024]{2,1,0:T(8,128)(2,1)} %param.15) | copy-start | bytes 6291460
  0.0 8.3 %copy-start.8 = (bf16[2048,512]{1,0:T(8,128)(2,1)S(1)}, bf16[2048,512]{1,0:T(8,128)(2,1)}, u32[]{:S(2)}) copy-start(bf16[2048,512]{1,0:T(8,128)(2,1)} %wf.1) | copy-start | bytes 6291460
  0.0 8.3 %copy-start.11 = (f32[1024,4]{0,1:T(4,128)S(1)}, f32[1024,4]{0,1:T(4,128)}, u32[]{:S(2)}) copy-start(f32[1024,4]{0,1:T(4,128)} %param.24) | copy-start | bytes 49156
  0.0 8.3 %copy-start.12 = (f32[512]{0:T(512)S(1)}, f32[512]{0:T(512)}, u32[]{:S(2)}) copy-start(f32[512]{0:T(512)} %param.23) | copy-start | bytes 6148
  0.0 8.3 %collective-permute-start = (bf16[1024,1024]{1,0:T(8,128)(2,1)}, bf16[1024,1024]{1,0:T(8,128)(2,1)S(1)}, u32[]{:S(2)}, u32[]{:S(2)}) collective-permute-start(bf16[1024,1024]{1,0:T(8,128)(2,1)} %bitcast.8), channel_id=1, source_target_pairs={{0,1},{1,0},{2,3},{3,2},{4,5},{5,4},{6,7},{7,6},{8,9},{9,8},{10,11... | collective-permute-start | bytes 6291464 | tf_op jit(solution)/shard_map/ppermute | solution.py:353
  1.5 39.9 %collective-permute-start.8 = (bf16[512,2048]{1,0:T(8,128)(2,1)}, bf16[512,2048]{1,0:T(8,128)(2,1)S(1)}, u32[]{:S(2)}, u32[]{:S(2)}) collective-permute-start(bf16[512,2048]{1,0:T(8,128)(2,1)} %wo.3), channel_id=1, source_target_pairs={{0,1},{1,0},{2,3},{3,2},{4,5},{5,4},{6,7},{7,6},{8,9},{9,8},{10,11... | collective-permute-start | bytes 6291464 | tf_op jit(solution)/shard_map/ppermute | solution.py:467
  2.7 4.3 %collective-permute-start.2 = (bf16[16,1024]{1,0:T(8,128)(2,1)S(1)}, bf16[16,1024]{1,0:T(8,128)(2,1)S(1)}, u32[]{:S(2)}, u32[]{:S(2)}) collective-permute-start(bf16[16,1024]{1,0:T(8,128)(2,1)S(1)} %shard_map.146), channel_id=1, source_target_pairs={{0,8},{8,16},{16,24},{24,32},{32,40},{40,48},{48,56},{56,64},{64,7... | collective-permute-start | bytes 98312 | tf_op jit(solution)/shard_map/ppermute | solution.py:354
  6.0 44.1 %collective-permute-start.10 = (bf16[512,2048]{1,0:T(8,128)(2,1)S(1)}, bf16[512,2048]{1,0:T(8,128)(2,1)S(1)}, u32[]{:S(2)}, u32[]{:S(2)}) collective-permute-start(bf16[512,2048]{1,0:T(8,128)(2,1)S(1)} %copy-done.1), channel_id=1, source_target_pairs={{0,1},{1,0},{2,3},{3,2},{4,5},{5,4},{6,7},{7,6},{8,9},{9,8},{10,11... | collective-permute-start | bytes 6291464 | tf_op jit(solution)/shard_map/ppermute | solution.py:468
  7.0 9.8 %collective-permute-start.3 = (bf16[16,1024]{1,0:T(8,128)(2,1)S(1)}, bf16[16,1024]{1,0:T(8,128)(2,1)S(1)}, u32[]{:S(2)}, u32[]{:S(2)}) collective-permute-start(bf16[16,1024]{1,0:T(8,128)(2,1)S(1)} %collective-permute-done.2.to), channel_id=1, source_target_pairs={{0,1},{1,0},{2,3},{3,2},{4,5},{5,4},{6,7},{7,6},{8,9},{9,8},{10,11... | collective-permute-start | bytes 98312 | tf_op jit(solution)/shard_map/ppermute | solution.py:355
  8.3 8.5 %copy-start.9 = (bf16[2048,512]{1,0:T(8,128)(2,1)S(1)}, bf16[2048,512]{1,0:T(8,128)(2,1)}, u32[]{:S(2)}) copy-start(bf16[2048,512]{1,0:T(8,128)(2,1)} %w.3) | copy-start | bytes 6291460
  8.3 8.5 %copy-start.10 = (bf16[2,256,256]{2,1,0:T(8,128)(2,1)S(1)}, bf16[2,256,256]{2,1,0:T(8,128)(2,1)}, u32[]{:S(2)}) copy-start(bf16[2,256,256]{2,1,0:T(8,128)(2,1)} %mix.1) | copy-start | bytes 786436
  8.3 8.5 %copy-start.13 = (f32[512]{0:T(512)S(1)}, f32[512]{0:T(512)}, u32[]{:S(2)}) copy-start(f32[512]{0:T(512)} %param.22) | copy-start | bytes 6148
  16.8 11.7 %copy-start.2 = (bf16[2048,512]{1,0:T(8,128)(2,1)S(1)}, bf16[2048,512]{1,0:T(8,128)(2,1)}, u32[]{:S(2)}) copy-start(bf16[2048,512]{1,0:T(8,128)(2,1)} %w.4) | copy-start | bytes 6291460
  20.1 21.2 %collective-permute-start.7 = (bf16[1024,512]{1,0:T(8,128)(2,1)S(1)}, bf16[1024,512]{1,0:T(8,128)(2,1)S(1)}, u32[]{:S(2)}, u32[]{:S(2)}) collective-permute-start(bf16[1024,512]{1,0:T(8,128)(2,1)S(1)} %shard_map.147.po), channel_id=1, source_target_pairs={{0,1},{1,0},{2,3},{3,2},{4,5},{5,4},{6,7},{7,6},{8,9},{9,8},{10,11... | collective-permute-start | bytes 3145736 | tf_op jit(solution)/shard_map/ppermute | solution.py:434
  20.2 5.7 %collective-permute-start.1 = (bf16[528,128]{1,0:T(8,128)(2,1)S(1)}, bf16[528,128]{1,0:T(8,128)(2,1)S(1)}, u32[]{:S(2)}, u32[]{:S(2)}) collective-permute-start(bf16[528,128]{1,0:T(8,128)(2,1)S(1)} %get-tuple-element.40), channel_id=1, source_target_pairs={{0,8},{8,0},{16,24},{24,16},{1,9},{9,1},{17,25},{25,17},{2,10},{10... | collective-permute-start | bytes 405512 | tf_op jit(solution)/shard_map/ppermute | solution.py:419
  26.0 5.9 %collective-permute-start.4 = (bf16[528,128]{1,0:T(8,128)(2,1)S(1)}, bf16[528,128]{1,0:T(8,128)(2,1)S(1)}, u32[]{:S(2)}, u32[]{:S(2)}) collective-permute-start(bf16[528,128]{1,0:T(8,128)(2,1)S(1)} %get-tuple-element.45), channel_id=1, source_target_pairs={{0,24},{24,0},{8,16},{16,8},{1,25},{25,1},{9,17},{17,9},{2,26},{26... | collective-permute-start | bytes 405512 | tf_op jit(solution)/shard_map/ppermute | solution.py:438
  28.5 6.5 %copy-start.3 = (bf16[2048,512]{1,0:T(8,128)(2,1)S(1)}, bf16[2048,512]{1,0:T(8,128)(2,1)}, u32[]{:S(2)}) copy-start(bf16[2048,512]{1,0:T(8,128)(2,1)} %w.5) | copy-start | bytes 6291460
  28.5 6.5 %copy-start.7 = (f32[128]{0:T(128)S(1)}, f32[128]{0:T(128)}, u32[]{:S(2)}) copy-start(f32[128]{0:T(128)} %param.25) | copy-start | bytes 1540
  32.0 5.6 %collective-permute-start.5 = (bf16[528,128]{1,0:T(8,128)(2,1)S(1)}, bf16[528,128]{1,0:T(8,128)(2,1)S(1)}, u32[]{:S(2)}, u32[]{:S(2)}) collective-permute-start(bf16[528,128]{1,0:T(8,128)(2,1)S(1)} %get-tuple-element.53), channel_id=1, source_target_pairs={{0,32},{32,0},{64,96},{96,64},{1,33},{33,1},{65,97},{97,65},{2,34}... | collective-permute-start | bytes 405512 | tf_op jit(solution)/shard_map/ppermute | solution.py:452
  35.0 6.3 %copy-start.4 = (bf16[512,2048]{1,0:T(8,128)(2,1)S(1)}, bf16[512,2048]{1,0:T(8,128)(2,1)}, u32[]{:S(2)}) copy-start(bf16[512,2048]{1,0:T(8,128)(2,1)} %wo.3) | copy-start | bytes 6291460
  37.7 6.1 %collective-permute-start.6 = (bf16[528,128]{1,0:T(8,128)(2,1)S(1)}, bf16[528,128]{1,0:T(8,128)(2,1)S(1)}, u32[]{:S(2)}, u32[]{:S(2)}) collective-permute-start(bf16[528,128]{1,0:T(8,128)(2,1)S(1)} %get-tuple-element.56), channel_id=1, source_target_pairs={{0,96},{96,0},{32,64},{64,32},{1,97},{97,1},{33,65},{65,33},{2,98}... | collective-permute-start | bytes 405512 | tf_op jit(solution)/shard_map/ppermute | solution.py:466
  44.6 6.1 %collective-permute-start.12 = (bf16[512,512]{1,0:T(8,128)(2,1)S(1)}, bf16[512,512]{1,0:T(8,128)(2,1)S(1)}, u32[]{:S(2)}, u32[]{:S(2)}) collective-permute-start(bf16[512,512]{1,0:T(8,128)(2,1)S(1)} %shard_map.156.ro), channel_id=1, source_target_pairs={{0,1},{1,0},{2,3},{3,2},{4,5},{5,4},{6,7},{7,6},{8,9},{9,8},{10,11... | collective-permute-start | bytes 1572872 | tf_op jit(solution)/shard_map/ppermute | solution.py:515
  50.0 2.7 %collective-permute-start.9 = (bf16[512,512]{1,0:T(8,128)(2,1)S(1)}, bf16[512,512]{1,0:T(8,128)(2,1)S(1)}, u32[]{:S(2)}, u32[]{:S(2)}) collective-permute-start(bf16[512,512]{1,0:T(8,128)(2,1)S(1)} %shard_map.154.ro), channel_id=1, source_target_pairs={{0,1},{1,0},{2,3},{3,2},{4,5},{5,4},{6,7},{7,6},{8,9},{9,8},{10,11... | collective-permute-start | bytes 1572872 | tf_op jit(solution)/shard_map/ppermute | solution.py:515
  52.3 2.3 %copy-start.5 = (f32[1024]{0:T(1024)S(1)}, f32[1024]{0:T(1024)}, u32[]{:S(2)}) copy-start(f32[1024]{0:T(1024)} %param.28) | copy-start | bytes 12292
  52.3 2.3 %copy-start.6 = (f32[1024]{0:T(1024)S(1)}, f32[1024]{0:T(1024)}, u32[]{:S(2)}) copy-start(f32[1024]{0:T(1024)} %param.29) | copy-start | bytes 12292
  52.3 2.3 %collective-permute-start.13 = (f32[512,128]{1,0:T(8,128)S(1)}, f32[512,128]{1,0:T(8,128)S(1)}, u32[]{:S(2)}, u32[]{:S(2)}) collective-permute-start(f32[512,128]{1,0:T(8,128)S(1)} %get-tuple-element.72.own), channel_id=1, source_target_pairs={{0,1},{1,0},{2,3},{3,2},{4,5},{5,4},{6,7},{7,6},{8,9},{9,8},{10,11... | collective-permute-start | bytes 786440 | tf_op jit(solution)/shard_map/ppermute | solution.py:532
  54.3 1.7 %collective-permute-start.11 = (f32[512,128]{1,0:T(8,128)S(1)}, f32[512,128]{1,0:T(8,128)S(1)}, u32[]{:S(2)}, u32[]{:S(2)}) collective-permute-start(f32[512,128]{1,0:T(8,128)S(1)} %get-tuple-element.69.own), channel_id=1, source_target_pairs={{0,1},{1,0},{2,3},{3,2},{4,5},{5,4},{6,7},{7,6},{8,9},{9,8},{10,11... | collective-permute-start | bytes 786440 | tf_op jit(solution)/shard_map/ppermute | solution.py:542

commit v2 on v1

--- a/solution.py
+++ b/solution.py
@@ -86,30 +86,30 @@
     out[...] = x[...]
 
 
-def gates_body(
-    heads, xo, xp, wf, wv_far, lb, ed, v_out, down_out, rel_out, st_out, c_out, pay_out, own_out, state, off, wv, sem
-):
+def half_rows(ref, which):
+    half = ref.shape[0] // 2
+    return ref[pl.ds(pl.multiple_of(which * half, half), half), :]
+
+
+def part_body(xo, wf, out):
+    out[...] = mm(xo[...], half_rows(wf, lax.axis_index("tp")))
+
+
+def value_body(xo, xp, w, out):
+    out[...] = mm(side(xo[...], xp[...]), own_then_other(w)).astype(BF16)
+
+
+def gates_body(heads, part, xp, wf, v, lb, ed, down_out, rel_out, st_out, c_out, pay_out, own_out, state, off):
     i = pl.program_id(0)
-    rows = xo.shape[0]
+    rows = xp.shape[0]
     width = heads * DK
-
-    load = pltpu.make_async_copy(wv_far, wv, sem)
 
     @pl.when(i == 0)
     def _():
-        load.start()
         state[...] = jnp.zeros_like(state)
         off[...] = jnp.zeros_like(off)
 
-    features = side(xo[...], xp[...])
-    f = mm(features, own_then_other(wf)).astype(BF16).astype(F32)
-
-    @pl.when(i == 0)
-    def _():
-        load.wait()
-
-    v = mm(features, own_then_other(wv)).astype(BF16)
-    v_out[...] = v
+    f = (part[...] + mm(xp[...], half_rows(wf, 1 - lax.axis_index("tp")))).astype(BF16).astype(F32)
     low = lb[...]
     gap = 1.0 - low
     sig = jax.nn.sigmoid(f)
@@ -334,7 +334,7 @@
     heads = width // DK
     blocks = length // BLOCK
     pool_width = w_pool_in.shape[1]
-    tile_gates, tile_pool, tile_query, tile_gate, tile_base = 512, 1024, 1024, 1024, 1024
+    tile_gates, tile_pool, tile_query, tile_gate, tile_base = 1024, 1024, 1024, 1024, 1024
     sp_n = lax.axis_size(SP)
     tail = call(
         tail_body,
@@ -358,25 +358,35 @@
     halves = lambda rows: [rows_spec(rows, half), rows_spec(rows, half)]
     full_w = lambda cols: [whole((D, cols))]
     state_rows = blocks * width
-    v, down, rel, st, cfac, pay, own = call(
+    f_part = call(
+        part_body,
+        (xo, w_forget),
+        [whole((length, half)), whole((D, width))],
+        whole((length, width)),
+        shape(length, width, F32),
+        (1,),
+        flops=full_flops // 2,
+    )
+    v = call(
+        value_body,
+        (xo, xp, w_value),
+        halves(length) + full_w(width),
+        whole((length, width)),
+        shape(length, width, BF16),
+        (1,),
+        flops=full_flops,
+    )
+    down, rel, st, cfac, pay, own = call(
         functools.partial(gates_body, heads),
-        (
-            xo,
-            xp,
-            w_forget,
-            pltpu.with_memory_space_constraint(w_value, pltpu.HBM),
-            lower_bound.reshape(1, width),
-            extra_decay.T,
-        ),
-        halves(tile_gates)
+        (f_part, xp, w_forget, v, lower_bound.reshape(1, width), extra_decay.T),
+        [rows_spec(tile_gates, width), rows_spec(tile_gates, half)]
         + full_w(width)
         + [
-            pl.BlockSpec(memory_space=pl.ANY),
+            rows_spec(tile_gates, width),
             whole((1, width)),
             pl.BlockSpec((heads, tile_gates), lambda i: (0, i)),
         ],
         [
-            rows_spec(tile_gates, width),
             rows_spec(tile_gates, width),
             rows_spec(tile_gates, width),
             rows_spec(tile_gates // BLOCK * width, DK),
@@ -386,7 +396,6 @@
         ],
         [
             shape(length, width, BF16),
-            shape(length, width, BF16),
             shape(length, width, F32),
             shape(state_rows, DK, BF16),
             shape(blocks, width, F32),
@@ -394,20 +403,14 @@
             shape(width + 8, DK, F32),
         ],
         (length // tile_gates,),
-        scratch=[
-            pltpu.VMEM((width, DK), F32),
-            pltpu.VMEM((1, width), F32),
-            pltpu.VMEM((D, width), BF16),
-            pltpu.SemaphoreType.DMA,
-        ],
-        vmem=24,
-        flops=2 * full_flops,
+        scratch=[pltpu.VMEM((width, DK), F32), pltpu.VMEM((1, width), F32)],
+        flops=full_flops,
     )
 
     def combine(which, *args):
         return call(
             functools.partial(combine_body, heads, which),
-                args,
+            args,
             [whole((width + 8, DK))] * (len(args) - 1) + [whole((width + 16, DK))],
             [whole((width + 16, DK))] + [whole((width + 8, DK))] * (2 - which // 2),
             [shape(width + 16, DK, BF16)] + [shape(width + 8, DK, F32)] * (2 - which // 2),
@@ -489,7 +492,7 @@
         first = part * per
         rec = call(
             functools.partial(rec_body, heads, part * (blocks // parts)),
-                (
+            (
                 scores,
                 up1,
                 v,

time: 57.6 us -> 55.8 us (0.969)
  starting transfers between devices: 23.6 us -> 22.6 us
  Pallas kernels: 29.2 us -> 28.5 us
    ppermute x1, starting transfers between devices: 1.28 us -> 0.2 us  [layer(): tail_p = lax.ppermute(tail_o, 'tp', swap)]
    pallas_call x15 -> x17, Pallas kernels: 29.2 us -> 28.5 us  [call(): pl.pallas_call(body, grid=grid, in_specs=in_specs, out_specs=out_specs, s...]
  transfers between devices with their start and end apart: 14 -> 14, of which waited for: 3 -> 2; matrix products, arithmetic and copies ran while one was open for 0% -> 0% of each run, Pallas kernels for 48% -> 49%
where the time goes in v2:
time: 55.8 us; the launch traced here: 55.6 us
  Pallas kernels  28.5 us (51%)
  starting transfers between devices  22.6 us (41%)
  waiting for transfers between devices  4.18 us (7%)
    pallas_call x17, Pallas kernels, call(): pl.pallas_call(body, grid=grid, in_specs=in_specs, out_specs=out_specs, s...  28.5 us
    ppermute x2, starting transfers between devices, layer(): others.append(lax.ppermute(rec, 'tp', swap))  4.61 us
    ppermute x1, waiting for transfers between devices, layer(): got1 = lax.ppermute(pay, 'sp_1', pairs)  3.55 us
    ppermute x1, starting transfers between devices, layer(): got4 = lax.ppermute(pay4, 'sp_0', mirror)  3.48 us
    ppermute x1, starting transfers between devices, layer(): tail_o = lax.ppermute(tail, SP, [(i, i + 1) for i in range(sp_n - 1)])  3.46 us
    ppermute x1, starting transfers between devices, layer(): got3 = lax.ppermute(pay3, 'sp_0', pairs)  3.21 us
    ppermute x1, starting transfers between devices, layer(): got2 = lax.ppermute(pay2, 'sp_1', mirror)  2.54 us
    ppermute x1, starting transfers between devices, layer(): got1 = lax.ppermute(pay, 'sp_1', pairs)  1.74 us
  transfers between devices with their start and end apart: 14, of which 2 were waited for; matrix products, arithmetic and copies ran while one was open for 0% of the time, Pallas kernels for 49%

profile of v2, /device:TPU:1, one launch (start us, length us, event | category | flops | bytes accessed | tf_op | source)
XLA Modules:
  0.0 55.6 jit_solution(4470448225086937808)
XLA Ops:
  0.0 1.4 %collective-permute-start = (bf16[1024,1024]{1,0:T(8,128)(2,1)}, bf16[1024,1024]{1,0:T(8,128)(2,1)S(1)}, u32[]{:S(2)}, u32[]{:S(2)}) collective-permute-start(bf16[1024,1024]{1,0:T(8,128)(2,1)} %bitcast.8), channel_id=1, source_target_pairs={{0,1},{1,0},{2,3},{3,2},{4,5},{5,4},{6,7},{7,6},{8,9},{9,8},{10,11... | collective-permute-start | bytes 6291464 | tf_op jit(solution)/shard_map/ppermute | solution.py:353
  1.4 0.1 collective-permute-start.8
  1.5 1.2 %shard_map.148 = bf16[16,1024]{1,0:T(8,128)(2,1)S(1)} custom-call(bf16[1024,1024]{1,0:T(8,128)(2,1)} %bitcast.9), custom_call_target="tpu_custom_call" | custom-call | flops 2147483648 | bytes 2097152 | tf_op jit(solution)/shard_map/pallas_call | solution.py:36
  2.6 3.5 %collective-permute-start.2 = (bf16[16,1024]{1,0:T(8,128)(2,1)S(1)}, bf16[16,1024]{1,0:T(8,128)(2,1)S(1)}, u32[]{:S(2)}, u32[]{:S(2)}) collective-permute-start(bf16[16,1024]{1,0:T(8,128)(2,1)S(1)} %shard_map.148), channel_id=1, source_target_pairs={{0,8},{8,16},{16,24},{24,32},{32,40},{40,48},{48,56},{56,64},{64,7... | collective-permute-start | bytes 98312 | tf_op jit(solution)/shard_map/ppermute | solution.py:354
  6.1 0.8 %collective-permute-start.10 = (bf16[512,2048]{1,0:T(8,128)(2,1)S(1)}, bf16[512,2048]{1,0:T(8,128)(2,1)S(1)}, u32[]{:S(2)}, u32[]{:S(2)}) collective-permute-start(bf16[512,2048]{1,0:T(8,128)(2,1)S(1)} %copy-done.1), channel_id=1, source_target_pairs={{0,1},{1,0},{2,3},{3,2},{4,5},{5,4},{6,7},{7,6},{8,9},{9,8},{10,11... | collective-permute-start | bytes 6291464 | tf_op jit(solution)/shard_map/ppermute | solution.py:471
  6.9 1.2 %shard_map.145.part = f32[1024,512]{1,0:T(8,128)S(1)} custom-call(bf16[1024,1024]{1,0:T(8,128)(2,1)S(1)} %bitcast.10, bf16[2048,512]{1,0:T(8,128)(2,1)S(1)} %copy-done.2), custom_call_target="tpu_custom_call" | custom-call | flops 1073741824 | bytes 4194304 | tf_op jit(solution)/shard_map/pallas_call | solution.py:36
  8.1 0.0 copy-start.12
  8.2 0.0 copy-start.13
  8.2 0.0 collective-permute-done.2.to
  8.2 0.2 collective-permute-start.3
  8.4 0.0 collective-permute-done.xp
  8.4 2.3 %shard_map.146.v = bf16[1024,512]{1,0:T(8,128)(2,1)S(1)} custom-call(bf16[1024,1024]{1,0:T(8,128)(2,1)S(1)} %bitcast.11, bf16[1024,1024]{1,0:T(8,128)(2,1)S(1)} %collective-permute-done.xp, bf16[2048,512]{1,0:T(8,128)(2,1)S(1)} %copy-done.9), custom_call_target="tpu_custom_call" | custom-call | flops 2147483648 | bytes 6291456 | tf_op jit(solution)/shard_map/pallas_call | solution.py:36
  10.7 0.0 copy-start.10
  10.8 0.0 copy-start.11
  10.8 0.0 copy-start.14
  10.8 4.2 %shard_map.147 = (bf16[1024,512]{1,0:T(8,128)(2,1)S(1)}, f32[1024,512]{1,0:T(8,128)S(1)}, bf16[4096,128]{1,0:T(8,128)(2,1)S(1)}, f32[8,512]{1,0:T(8,128)S(1)}, b...) custom-call(f32[1024,512]{1,0:T(8,128)S(1)} %shard_map.145.part, bf16[1024,1024]{1,0:T(8,128)(2,1)S(1)} %collective-permute-done.xp, ...), custom_call_target="tpu_custom_call" | custom-call | flops 2147483648 | bytes 7358464 | tf_op jit(solution)/shard_map/pallas_call | solution.py:36
  15.0 0.0 collective-permute-done.3.tp
  15.0 0.0 copy-start.3
  15.0 3.3 %shard_map.149.po = bf16[1024,512]{1,0:T(8,128)(2,1)S(1)} custom-call(bf16[1024,1024]{1,0:T(8,128)(2,1)S(1)} %bitcast.12, bf16[1024,1024]{1,0:T(8,128)(2,1)S(1)} %collective-permute-done.xp, bf16[16,1024]{1,0:T(8,128)(2,1)S(1)} %collective-permute-done.2.to, bf16[16,1024]{1,0:T(8,128)(2,1)S(1)} %collective-permute-done.3.tp, ...), custom_call_target="tpu_custom_call" | custom-call | flops 2147483648 | bytes 6621184 | tf_op jit(solution)/shard_map/pallas_call | solution.py:36
  18.4 0.5 collective-permute-start.7
  18.8 1.7 %collective-permute-start.1 = (bf16[528,128]{1,0:T(8,128)(2,1)S(1)}, bf16[528,128]{1,0:T(8,128)(2,1)S(1)}, u32[]{:S(2)}, u32[]{:S(2)}) collective-permute-start(bf16[528,128]{1,0:T(8,128)(2,1)S(1)} %get-tuple-element.39), channel_id=1, source_target_pairs={{0,8},{8,0},{16,24},{24,16},{1,9},{9,1},{17,25},{25,17},{2,10},{10... | collective-permute-start | bytes 405512 | tf_op jit(solution)/shard_map/ppermute | solution.py:422
  20.6 3.5 %collective-permute-done.1.refs_0_ = bf16[528,128]{1,0:T(8,128)(2,1)S(1)} collective-permute-done((bf16[528,128]{1,0:T(8,128)(2,1)S(1)}, bf16[528,128]{1,0:T(8,128)(2,1)S(1)}, u32[]{:S(2)}, u32[]{:S(2)}) %collective-permute-start.1) | collective-permute-done | bytes 135200 | tf_op jit(solution)/shard_map/ppermute | solution.py:422
  24.1 0.1 shard_map.150
  24.2 2.5 %collective-permute-start.4 = (bf16[528,128]{1,0:T(8,128)(2,1)S(1)}, bf16[528,128]{1,0:T(8,128)(2,1)S(1)}, u32[]{:S(2)}, u32[]{:S(2)}) collective-permute-start(bf16[528,128]{1,0:T(8,128)(2,1)S(1)} %get-tuple-element.44), channel_id=1, source_target_pairs={{0,24},{24,0},{8,16},{16,8},{1,25},{25,1},{9,17},{17,9},{2,26},{26... | collective-permute-start | bytes 405512 | tf_op jit(solution)/shard_map/ppermute | solution.py:441
  26.7 3.4 %shard_map.151 = (bf16[1024,512]{1,0:T(8,128)(2,1)S(1)}, bf16[1024,512]{1,0:T(8,128)(2,1)S(1)}) custom-call(bf16[1024,1024]{1,0:T(8,128)(2,1)S(1)} %bitcast.13, bf16[1024,1024]{1,0:T(8,128)(2,1)S(1)} %collective-permute-done.xp, bf16[2048,512]{1,0:T(8,128)(2,1)S(1)} %copy-done.3, f32[1024,512]{1,0:T(8,128)S(1)} %get-tuple-element.46.rel, ...), custom_call_target="tpu_custom_call" | custom-call | flops 2147483648 | bytes 9437184 | tf_op jit(solution)/shard_map/pallas_call | solution.py:36
  30.1 0.0 collective-permute-done.4.refs_1_
  30.1 0.1 shard_map.152
  30.2 3.2 %collective-permute-start.5 = (bf16[528,128]{1,0:T(8,128)(2,1)S(1)}, bf16[528,128]{1,0:T(8,128)(2,1)S(1)}, u32[]{:S(2)}, u32[]{:S(2)}) collective-permute-start(bf16[528,128]{1,0:T(8,128)(2,1)S(1)} %get-tuple-element.52), channel_id=1, source_target_pairs={{0,32},{32,0},{64,96},{96,64},{1,33},{33,1},{65,97},{97,65},{2,34}... | collective-permute-start | bytes 405512 | tf_op jit(solution)/shard_map/ppermute | solution.py:455
  33.4 2.5 %shard_map.153.gate = f32[1024,512]{1,0:T(8,128)S(1)} custom-call(bf16[1024,1024]{1,0:T(8,128)(2,1)S(1)} %bitcast.14, bf16[1024,1024]{1,0:T(8,128)(2,1)S(1)} %collective-permute-done.xp, bf16[2048,512]{1,0:T(8,128)(2,1)S(1)} %copy-done.4, f32[1,128]{1,0:T(1,128)S(1)} %bitcast.20), custom_call_target="tpu_custom_call" | custom-call | flops 2147483648 | bytes 6291968 | tf_op jit(solution)/shard_map/pallas_call | solution.py:36
  36.0 0.0 collective-permute-done.5.refs_1_
  36.0 0.1 shard_map.154
  36.1 3.5 %collective-permute-start.6 = (bf16[528,128]{1,0:T(8,128)(2,1)S(1)}, bf16[528,128]{1,0:T(8,128)(2,1)S(1)}, u32[]{:S(2)}, u32[]{:S(2)}) collective-permute-start(bf16[528,128]{1,0:T(8,128)(2,1)S(1)} %get-tuple-element.55), channel_id=1, source_target_pairs={{0,96},{96,0},{32,64},{64,32},{1,97},{97,1},{33,65},{65,33},{2,98}... | collective-permute-start | bytes 405512 | tf_op jit(solution)/shard_map/ppermute | solution.py:469
  39.6 0.0 collective-permute-done.8.wp
  39.6 0.0 collective-permute-done.7.pp
  39.6 2.4 %shard_map.155.base = f32[1024,1024]{1,0:T(8,128)S(1)} custom-call(bf16[1024,1024]{1,0:T(8,128)(2,1)S(1)} %bitcast.15, bf16[1024,512]{1,0:T(8,128)(2,1)S(1)} %shard_map.149.po, bf16[1024,512]{1,0:T(8,128)(2,1)S(1)} %collective-permute-done.7.pp, bf16[512,2048]{1,0:T(8,128)(2,1)S(1)} %copy-done.5, bf16[512,2048]{1,0:T(8,128)(2,1)S(1)} %collective-permute-done.8.wp), custom_call_target="tpu_custom_call" | custom-call | flops 2147483648 | bytes 8388608 | tf_op jit(solution)/shard_map/pallas_call | solution.py:36
  42.0 0.0 collective-permute-done.6.recv
  42.0 0.8 %shard_map.158.ro = bf16[512,512]{1,0:T(8,128)(2,1)S(1)} custom-call(bf16[1024,512]{1,0:T(8,128)(2,1)S(1)} %get-tuple-element.59.scores, bf16[1024,512]{1,0:T(8,128)(2,1)S(1)} %get-tuple-element.60.up, bf16[1024,512]{1,0:T(8,128)(2,1)S(1)} %shard_map.146.v, f32[1024,512]{1,0:T(8,128)S(1)} %shard_map.153.gate, bf16[4096,128]{1,0:T(8,128)(2,1)S(1)} %get-tuple-element.62.st, ...), custom_call_target="tpu_custom_call" | custom-call | flops 536870912 | bytes 6709248 | tf_op jit(solution)/shard_map/pallas_call | solution.py:36
  42.8 4.5 %collective-permute-start.12 = (bf16[512,512]{1,0:T(8,128)(2,1)S(1)}, bf16[512,512]{1,0:T(8,128)(2,1)S(1)}, u32[]{:S(2)}, u32[]{:S(2)}) collective-permute-start(bf16[512,512]{1,0:T(8,128)(2,1)S(1)} %shard_map.158.ro), channel_id=1, source_target_pairs={{0,1},{1,0},{2,3},{3,2},{4,5},{5,4},{6,7},{7,6},{8,9},{9,8},{10,11... | collective-permute-start | bytes 1572872 | tf_op jit(solution)/shard_map/ppermute | solution.py:518
  47.4 0.8 %shard_map.156.ro = bf16[512,512]{1,0:T(8,128)(2,1)S(1)} custom-call(bf16[1024,512]{1,0:T(8,128)(2,1)S(1)} %get-tuple-element.59.scores, bf16[1024,512]{1,0:T(8,128)(2,1)S(1)} %get-tuple-element.60.up, bf16[1024,512]{1,0:T(8,128)(2,1)S(1)} %shard_map.146.v, f32[1024,512]{1,0:T(8,128)S(1)} %shard_map.153.gate, bf16[4096,128]{1,0:T(8,128)(2,1)S(1)} %get-tuple-element.62.st, ...), custom_call_target="tpu_custom_call" | custom-call | flops 536870912 | bytes 6709248 | tf_op jit(solution)/shard_map/pallas_call | solution.py:36
  48.2 0.1 collective-permute-start.9
  48.3 0.0 collective-permute-done.10.wp
  48.3 0.6 %collective-permute-done.12.rp = bf16[512,512]{1,0:T(8,128)(2,1)S(1)} collective-permute-done((bf16[512,512]{1,0:T(8,128)(2,1)S(1)}, bf16[512,512]{1,0:T(8,128)(2,1)S(1)}, u32[]{:S(2)}, u32[]{:S(2)}) %collective-permute-start.12) | collective-permute-done | bytes 524320 | tf_op jit(solution)/shard_map/ppermute | solution.py:518
  48.9 1.6 %shard_map.159 = (f32[512,1024]{1,0:T(8,128)S(1)}, f32[512,128]{1,0:T(8,128)S(1)}) custom-call(f32[1024,1024]{1,0:T(8,128)S(1)} %shard_map.155.base, bf16[512,512]{1,0:T(8,128)(2,1)S(1)} %shard_map.158.ro, bf16[512,512]{1,0:T(8,128)(2,1)S(1)} %collective-permute-done.12.rp, bf16[512,2048]{1,0:T(8,128)(2,1)S(1)} %copy-done.1, ...), custom_call_target="tpu_custom_call" | custom-call | flops 1073741824 | bytes 9437184 | tf_op jit(solution)/shard_map/pallas_call | solution.py:36
  50.5 0.5 collective-permute-start.13
  50.9 1.6 %shard_map.157 = (f32[512,1024]{1,0:T(8,128)S(1)}, f32[512,128]{1,0:T(8,128)S(1)}) custom-call(f32[1024,1024]{1,0:T(8,128)S(1)} %shard_map.155.base, bf16[512,512]{1,0:T(8,128)(2,1)S(1)} %shard_map.156.ro, bf16[512,512]{1,0:T(8,128)(2,1)S(1)} %collective-permute-done.9.rp, bf16[512,2048]{1,0:T(8,128)(2,1)S(1)} %copy-done.1, ...), custom_call_target="tpu_custom_call" | custom-call | flops 1073741824 | bytes 9437184 | tf_op jit(solution)/shard_map/pallas_call | solution.py:36
  52.5 0.2 collective-permute-start.11
  52.7 1.5 %shard_map.160.before = bf16[1024,1024]{1,0:T(8,128)(2,1)} custom-call(f32[512,1024]{1,0:T(8,128)S(1)} %get-tuple-element.69.resid, f32[512,128]{1,0:T(8,128)S(1)} %get-tuple-element.70.own, f32[512,128]{1,0:T(8,128)S(1)} %collective-permute-done.13.other, f32[1,1024]{1,0:T(1,128)S(1)} %bitcast.16, f32[1,1024]{1,0:T(1,128)S(1)} %bitcast.18), custom_call_target="tpu_custom_call" | custom-call | flops 536870912 | bytes 2629632 | tf_op jit(solution)/shard_map/pallas_call | solution.py:36
  54.2 1.4 %shard_map.161 = bf16[1024,1024]{1,0:T(8,128)(2,1)} custom-call(f32[512,1024]{1,0:T(8,128)S(1)} %get-tuple-element.66.resid, f32[512,128]{1,0:T(8,128)S(1)} %get-tuple-element.67.own, f32[512,128]{1,0:T(8,128)S(1)} %collective-permute-done.11.other, f32[1,1024]{1,0:T(1,128)S(1)} %bitcast.17, f32[1,1024]{1,0:T(1,128)S(1)} %bitcast.19, ...), custom_call_target="tpu_custom_call", output_to_operand_aliasing={{}: (5, {})} | custom-call | flops 536870912 | bytes 4726784 | tf_op jit(solution)/shard_map/pallas_call | solution.py:36
  (27 shorter events, 0.1 us)
Async XLA Ops:
  0.0 6.1 %copy-start.1 = (bf16[512,2048]{1,0:T(8,128)(2,1)S(1)}, bf16[512,2048]{1,0:T(8,128)(2,1)}, u32[]{:S(2)}) copy-start(bf16[512,2048]{1,0:T(8,128)(2,1)} %wo.5) | copy-start | bytes 6291460
  0.0 6.9 %copy-start = (bf16[1,1024,1024]{2,1,0:T(8,128)(2,1)S(1)}, bf16[1,1024,1024]{2,1,0:T(8,128)(2,1)}, u32[]{:S(2)}) copy-start(bf16[1,1024,1024]{2,1,0:T(8,128)(2,1)} %param.15) | copy-start | bytes 6291460
  0.0 6.9 %copy-start.2 = (bf16[2048,512]{1,0:T(8,128)(2,1)S(1)}, bf16[2048,512]{1,0:T(8,128)(2,1)}, u32[]{:S(2)}) copy-start(bf16[2048,512]{1,0:T(8,128)(2,1)} %wf.3) | copy-start | bytes 6291460
  0.0 8.4 %collective-permute-start = (bf16[1024,1024]{1,0:T(8,128)(2,1)}, bf16[1024,1024]{1,0:T(8,128)(2,1)S(1)}, u32[]{:S(2)}, u32[]{:S(2)}) collective-permute-start(bf16[1024,1024]{1,0:T(8,128)(2,1)} %bitcast.8), channel_id=1, source_target_pairs={{0,1},{1,0},{2,3},{3,2},{4,5},{5,4},{6,7},{7,6},{8,9},{9,8},{10,11... | collective-permute-start | bytes 6291464 | tf_op jit(solution)/shard_map/ppermute | solution.py:353
  1.4 38.2 %collective-permute-start.8 = (bf16[512,2048]{1,0:T(8,128)(2,1)}, bf16[512,2048]{1,0:T(8,128)(2,1)S(1)}, u32[]{:S(2)}, u32[]{:S(2)}) collective-permute-start(bf16[512,2048]{1,0:T(8,128)(2,1)} %wo.3), channel_id=1, source_target_pairs={{0,1},{1,0},{2,3},{3,2},{4,5},{5,4},{6,7},{7,6},{8,9},{9,8},{10,11... | collective-permute-start | bytes 6291464 | tf_op jit(solution)/shard_map/ppermute | solution.py:470
  2.6 5.8 %copy-start.9 = (bf16[2048,512]{1,0:T(8,128)(2,1)S(1)}, bf16[2048,512]{1,0:T(8,128)(2,1)}, u32[]{:S(2)}) copy-start(bf16[2048,512]{1,0:T(8,128)(2,1)} %w.4) | copy-start | bytes 6291460
  2.6 5.5 %collective-permute-start.2 = (bf16[16,1024]{1,0:T(8,128)(2,1)S(1)}, bf16[16,1024]{1,0:T(8,128)(2,1)S(1)}, u32[]{:S(2)}, u32[]{:S(2)}) collective-permute-start(bf16[16,1024]{1,0:T(8,128)(2,1)S(1)} %shard_map.148), channel_id=1, source_target_pairs={{0,8},{8,16},{16,24},{24,32},{32,40},{40,48},{48,56},{56,64},{64,7... | collective-permute-start | bytes 98312 | tf_op jit(solution)/shard_map/ppermute | solution.py:354
  6.1 42.2 %collective-permute-start.10 = (bf16[512,2048]{1,0:T(8,128)(2,1)S(1)}, bf16[512,2048]{1,0:T(8,128)(2,1)S(1)}, u32[]{:S(2)}, u32[]{:S(2)}) collective-permute-start(bf16[512,2048]{1,0:T(8,128)(2,1)S(1)} %copy-done.1), channel_id=1, source_target_pairs={{0,1},{1,0},{2,3},{3,2},{4,5},{5,4},{6,7},{7,6},{8,9},{9,8},{10,11... | collective-permute-start | bytes 6291464 | tf_op jit(solution)/shard_map/ppermute | solution.py:471
  8.1 2.6 %copy-start.12 = (f32[1024,4]{0,1:T(4,128)S(1)}, f32[1024,4]{0,1:T(4,128)}, u32[]{:S(2)}) copy-start(f32[1024,4]{0,1:T(4,128)} %param.24) | copy-start | bytes 49156
  8.2 2.6 %copy-start.13 = (f32[512]{0:T(512)S(1)}, f32[512]{0:T(512)}, u32[]{:S(2)}) copy-start(f32[512]{0:T(512)} %param.23) | copy-start | bytes 6148
  8.2 6.8 %collective-permute-start.3 = (bf16[16,1024]{1,0:T(8,128)(2,1)S(1)}, bf16[16,1024]{1,0:T(8,128)(2,1)S(1)}, u32[]{:S(2)}, u32[]{:S(2)}) collective-permute-start(bf16[16,1024]{1,0:T(8,128)(2,1)S(1)} %collective-permute-done.2.to), channel_id=1, source_target_pairs={{0,1},{1,0},{2,3},{3,2},{4,5},{5,4},{6,7},{7,6},{8,9},{9,8},{10,11... | collective-permute-start | bytes 98312 | tf_op jit(solution)/shard_map/ppermute | solution.py:355
  10.7 4.3 %copy-start.10 = (bf16[2048,512]{1,0:T(8,128)(2,1)S(1)}, bf16[2048,512]{1,0:T(8,128)(2,1)}, u32[]{:S(2)}) copy-start(bf16[2048,512]{1,0:T(8,128)(2,1)} %w.5) | copy-start | bytes 6291460
  10.8 4.3 %copy-start.11 = (bf16[2,256,256]{2,1,0:T(8,128)(2,1)S(1)}, bf16[2,256,256]{2,1,0:T(8,128)(2,1)}, u32[]{:S(2)}) copy-start(bf16[2,256,256]{2,1,0:T(8,128)(2,1)} %mix.1) | copy-start | bytes 786436
  10.8 4.3 %copy-start.14 = (f32[512]{0:T(512)S(1)}, f32[512]{0:T(512)}, u32[]{:S(2)}) copy-start(f32[512]{0:T(512)} %param.22) | copy-start | bytes 6148
  15.0 11.7 %copy-start.3 = (bf16[2048,512]{1,0:T(8,128)(2,1)S(1)}, bf16[2048,512]{1,0:T(8,128)(2,1)}, u32[]{:S(2)}) copy-start(bf16[2048,512]{1,0:T(8,128)(2,1)} %w.6) | copy-start | bytes 6291460
  18.4 21.2 %collective-permute-start.7 = (bf16[1024,512]{1,0:T(8,128)(2,1)S(1)}, bf16[1024,512]{1,0:T(8,128)(2,1)S(1)}, u32[]{:S(2)}, u32[]{:S(2)}) collective-permute-start(bf16[1024,512]{1,0:T(8,128)(2,1)S(1)} %shard_map.149.po), channel_id=1, source_target_pairs={{0,1},{1,0},{2,3},{3,2},{4,5},{5,4},{6,7},{7,6},{8,9},{9,8},{10,11... | collective-permute-start | bytes 3145736 | tf_op jit(solution)/shard_map/ppermute | solution.py:437
  18.8 5.3 %collective-permute-start.1 = (bf16[528,128]{1,0:T(8,128)(2,1)S(1)}, bf16[528,128]{1,0:T(8,128)(2,1)S(1)}, u32[]{:S(2)}, u32[]{:S(2)}) collective-permute-start(bf16[528,128]{1,0:T(8,128)(2,1)S(1)} %get-tuple-element.39), channel_id=1, source_target_pairs={{0,8},{8,0},{16,24},{24,16},{1,9},{9,1},{17,25},{25,17},{2,10},{10... | collective-permute-start | bytes 405512 | tf_op jit(solution)/shard_map/ppermute | solution.py:422
  24.2 5.9 %collective-permute-start.4 = (bf16[528,128]{1,0:T(8,128)(2,1)S(1)}, bf16[528,128]{1,0:T(8,128)(2,1)S(1)}, u32[]{:S(2)}, u32[]{:S(2)}) collective-permute-start(bf16[528,128]{1,0:T(8,128)(2,1)S(1)} %get-tuple-element.44), channel_id=1, source_target_pairs={{0,24},{24,0},{8,16},{16,8},{1,25},{25,1},{9,17},{17,9},{2,26},{26... | collective-permute-start | bytes 405512 | tf_op jit(solution)/shard_map/ppermute | solution.py:441
  26.7 6.7 %copy-start.4 = (bf16[2048,512]{1,0:T(8,128)(2,1)S(1)}, bf16[2048,512]{1,0:T(8,128)(2,1)}, u32[]{:S(2)}) copy-start(bf16[2048,512]{1,0:T(8,128)(2,1)} %w.7) | copy-start | bytes 6291460
  26.7 6.7 %copy-start.8 = (f32[128]{0:T(128)S(1)}, f32[128]{0:T(128)}, u32[]{:S(2)}) copy-start(f32[128]{0:T(128)} %param.25) | copy-start | bytes 1540
  30.2 5.8 %collective-permute-start.5 = (bf16[528,128]{1,0:T(8,128)(2,1)S(1)}, bf16[528,128]{1,0:T(8,128)(2,1)S(1)}, u32[]{:S(2)}, u32[]{:S(2)}) collective-permute-start(bf16[528,128]{1,0:T(8,128)(2,1)S(1)} %get-tuple-element.52), channel_id=1, source_target_pairs={{0,32},{32,0},{64,96},{96,64},{1,33},{33,1},{65,97},{97,65},{2,34}... | collective-permute-start | bytes 405512 | tf_op jit(solution)/shard_map/ppermute | solution.py:455
  33.4 6.2 %copy-start.5 = (bf16[512,2048]{1,0:T(8,128)(2,1)S(1)}, bf16[512,2048]{1,0:T(8,128)(2,1)}, u32[]{:S(2)}) copy-start(bf16[512,2048]{1,0:T(8,128)(2,1)} %wo.3) | copy-start | bytes 6291460
  36.1 5.9 %collective-permute-start.6 = (bf16[528,128]{1,0:T(8,128)(2,1)S(1)}, bf16[528,128]{1,0:T(8,128)(2,1)S(1)}, u32[]{:S(2)}, u32[]{:S(2)}) collective-permute-start(bf16[528,128]{1,0:T(8,128)(2,1)S(1)} %get-tuple-element.55), channel_id=1, source_target_pairs={{0,96},{96,0},{32,64},{64,32},{1,97},{97,1},{33,65},{65,33},{2,98}... | collective-permute-start | bytes 405512 | tf_op jit(solution)/shard_map/ppermute | solution.py:469
  42.8 6.0 %collective-permute-start.12 = (bf16[512,512]{1,0:T(8,128)(2,1)S(1)}, bf16[512,512]{1,0:T(8,128)(2,1)S(1)}, u32[]{:S(2)}, u32[]{:S(2)}) collective-permute-start(bf16[512,512]{1,0:T(8,128)(2,1)S(1)} %shard_map.158.ro), channel_id=1, source_target_pairs={{0,1},{1,0},{2,3},{3,2},{4,5},{5,4},{6,7},{7,6},{8,9},{9,8},{10,11... | collective-permute-start | bytes 1572872 | tf_op jit(solution)/shard_map/ppermute | solution.py:518
  48.2 2.7 %collective-permute-start.9 = (bf16[512,512]{1,0:T(8,128)(2,1)S(1)}, bf16[512,512]{1,0:T(8,128)(2,1)S(1)}, u32[]{:S(2)}, u32[]{:S(2)}) collective-permute-start(bf16[512,512]{1,0:T(8,128)(2,1)S(1)} %shard_map.156.ro), channel_id=1, source_target_pairs={{0,1},{1,0},{2,3},{3,2},{4,5},{5,4},{6,7},{7,6},{8,9},{9,8},{10,11... | collective-permute-start | bytes 1572872 | tf_op jit(solution)/shard_map/ppermute | solution.py:518
  50.5 2.2 %copy-start.6 = (f32[1024]{0:T(1024)S(1)}, f32[1024]{0:T(1024)}, u32[]{:S(2)}) copy-start(f32[1024]{0:T(1024)} %param.28) | copy-start | bytes 12292
  50.5 2.2 %copy-start.7 = (f32[1024]{0:T(1024)S(1)}, f32[1024]{0:T(1024)}, u32[]{:S(2)}) copy-start(f32[1024]{0:T(1024)} %param.29) | copy-start | bytes 12292
  50.5 2.2 %collective-permute-start.13 = (f32[512,128]{1,0:T(8,128)S(1)}, f32[512,128]{1,0:T(8,128)S(1)}, u32[]{:S(2)}, u32[]{:S(2)}) collective-permute-start(f32[512,128]{1,0:T(8,128)S(1)} %get-tuple-element.70.own), channel_id=1, source_target_pairs={{0,1},{1,0},{2,3},{3,2},{4,5},{5,4},{6,7},{7,6},{8,9},{9,8},{10,11... | collective-permute-start | bytes 786440 | tf_op jit(solution)/shard_map/ppermute | solution.py:535
  52.5 1.7 %collective-permute-start.11 = (f32[512,128]{1,0:T(8,128)S(1)}, f32[512,128]{1,0:T(8,128)S(1)}, u32[]{:S(2)}, u32[]{:S(2)}) collective-permute-start(f32[512,128]{1,0:T(8,128)S(1)} %get-tuple-element.67.own), channel_id=1, source_target_pairs={{0,1},{1,0},{2,3},{3,2},{4,5},{5,4},{6,7},{7,6},{8,9},{9,8},{10,11... | collective-permute-start | bytes 786440 | tf_op jit(solution)/shard_map/ppermute | solution.py:545

commit v3 on v2

--- a/solution.py
+++ b/solution.py
@@ -12,6 +12,7 @@
 DK = 128
 BLOCK = 128
 MID = 63
+VALUE_ROWS = 1024
 HALO = 16
 GROUP_CH = 256
 SP = ("sp_0", "sp_1")
@@ -95,11 +96,7 @@
     out[...] = mm(xo[...], half_rows(wf, lax.axis_index("tp")))
 
 
-def value_body(xo, xp, w, out):
-    out[...] = mm(side(xo[...], xp[...]), own_then_other(w)).astype(BF16)
-
-
-def gates_body(heads, part, xp, wf, v, lb, ed, down_out, rel_out, st_out, c_out, pay_out, own_out, state, off):
+def gates_body(heads, part, xo, xp, wf, wv, lb, ed, v, down_out, rel_out, st_out, c_out, pay_out, own_out, state, off):
     i = pl.program_id(0)
     rows = xp.shape[0]
     width = heads * DK
@@ -128,6 +125,8 @@
     t_id = lax.broadcasted_iota(jnp.int32, (BLOCK, 2 * BLOCK), 0)
     s_id = lax.broadcasted_iota(jnp.int32, (BLOCK, 2 * BLOCK), 1)
     mask = (t_id >= jnp.where(s_id >= BLOCK, s_id - BLOCK, s_id)).astype(F32).astype(BF16)
+    per = VALUE_ROWS // BLOCK
+    weights = []
     for b in range(rows // BLOCK):
         r = slice(b * BLOCK, (b + 1) * BLOCK)
         total = mm(mask, jnp.concatenate([hi[r], lo[r]], axis=0))
@@ -137,16 +136,22 @@
         rel_out[r, :] = rel
         down = weight[r] * jnp.exp(-rel)
         down_out[r, :] = down.astype(BF16)
-        in_weight = (down * jnp.exp(end - middle)).astype(BF16)
-        e_mid, e_end = jnp.exp(middle), jnp.exp(end)
         before = off[...]
         c_out[pl.ds(i * (rows // BLOCK) + b, 1), :] = jnp.exp(middle + before)
         off[...] = before + end
-        for h in range(heads):
-            c = slice(h * DK, (h + 1) * DK)
-            old = state[c, :]
-            st_out[b * width + h * DK : b * width + (h + 1) * DK, :] = (old * e_mid[:, c]).astype(BF16)
-            state[c, :] = old * e_end[:, c] + mm_t(v[r, c], in_weight[:, c], 0, 0)
+        weights.append((b, (down * jnp.exp(end - middle)).astype(BF16), jnp.exp(middle), jnp.exp(end)))
+        if len(weights) < per:
+            continue
+        some = slice((b + 1 - per) * BLOCK, (b + 1) * BLOCK)
+        v[some, :] = mm(side(xo[some, :], xp[some, :]), own_then_other(wv)).astype(BF16)
+        for at, in_weight, e_mid, e_end in weights:
+            r = slice(at * BLOCK, (at + 1) * BLOCK)
+            for h in range(heads):
+                c = slice(h * DK, (h + 1) * DK)
+                old = state[c, :]
+                st_out[at * width + h * DK : at * width + (h + 1) * DK, :] = (old * e_mid[:, c]).astype(BF16)
+                state[c, :] = old * e_end[:, c] + mm_t(v[r, c], in_weight[:, c], 0, 0)
+        weights = []
 
     @pl.when(i == pl.num_programs(0) - 1)
     def _():
@@ -367,26 +372,18 @@
         (1,),
         flops=full_flops // 2,
     )
-    v = call(
-        value_body,
-        (xo, xp, w_value),
-        halves(length) + full_w(width),
-        whole((length, width)),
-        shape(length, width, BF16),
-        (1,),
-        flops=full_flops,
-    )
-    down, rel, st, cfac, pay, own = call(
+    v, down, rel, st, cfac, pay, own = call(
         functools.partial(gates_body, heads),
-        (f_part, xp, w_forget, v, lower_bound.reshape(1, width), extra_decay.T),
-        [rows_spec(tile_gates, width), rows_spec(tile_gates, half)]
-        + full_w(width)
+        (f_part, xo, xp, w_forget, w_value, lower_bound.reshape(1, width), extra_decay.T),
+        [rows_spec(tile_gates, width)]
+        + halves(tile_gates)
+        + full_w(width) * 2
         + [
-            rows_spec(tile_gates, width),
             whole((1, width)),
             pl.BlockSpec((heads, tile_gates), lambda i: (0, i)),
         ],
         [
+            rows_spec(tile_gates, width),
             rows_spec(tile_gates, width),
             rows_spec(tile_gates, width),
             rows_spec(tile_gates // BLOCK * width, DK),
@@ -395,6 +392,7 @@
             whole((width + 8, DK)),
         ],
         [
+            shape(length, width, BF16),
             shape(length, width, BF16),
             shape(length, width, F32),
             shape(state_rows, DK, BF16),

time: 55.8 us -> 54.3 us (0.973)
  Pallas kernels: 28.5 us -> 27 us
    pallas_call x17 -> x16, Pallas kernels: 28.5 us -> 27 us  [call(): pl.pallas_call(body, grid=grid, in_specs=in_specs, out_specs=out_specs, s...]
  transfers between devices with their start and end apart: 14 -> 14, of which waited for: 2 -> 2; matrix products, arithmetic and copies ran while one was open for 0% -> 0% of each run, Pallas kernels for 49% -> 47%
where the time goes in v3:
time: 54.3 us; the launch traced here: 54.2 us
  Pallas kernels  27 us (50%)
  starting transfers between devices  22.7 us (42%)
  waiting for transfers between devices  4.18 us (8%)
    pallas_call x16, Pallas kernels, call(): pl.pallas_call(body, grid=grid, in_specs=in_specs, out_specs=out_specs, s...  27 us
    ppermute x2, starting transfers between devices, layer(): others.append(lax.ppermute(rec, 'tp', swap))  4.63 us
    ppermute x1, waiting for transfers between devices, layer(): got1 = lax.ppermute(pay, 'sp_1', pairs)  3.55 us
    ppermute x1, starting transfers between devices, layer(): got4 = lax.ppermute(pay4, 'sp_0', mirror)  3.49 us
    ppermute x1, starting transfers between devices, layer(): tail_o = lax.ppermute(tail, SP, [(i, i + 1) for i in range(sp_n - 1)])  3.47 us
    ppermute x1, starting transfers between devices, layer(): got3 = lax.ppermute(pay3, 'sp_0', pairs)  3.24 us
    ppermute x1, starting transfers between devices, layer(): got2 = lax.ppermute(pay2, 'sp_1', mirror)  2.53 us
    ppermute x1, starting transfers between devices, layer(): got1 = lax.ppermute(pay, 'sp_1', pairs)  1.75 us
  transfers between devices with their start and end apart: 14, of which 2 were waited for; matrix products, arithmetic and copies ran while one was open for 0% of the time, Pallas kernels for 47%

profile of v3, /device:TPU:1, one launch (start us, length us, event | category | flops | bytes accessed | tf_op | source)
XLA Modules:
  0.0 54.2 jit_solution(2441321023346869269)
XLA Ops:
  0.0 1.4 %collective-permute-start = (bf16[1024,1024]{1,0:T(8,128)(2,1)}, bf16[1024,1024]{1,0:T(8,128)(2,1)S(1)}, u32[]{:S(2)}, u32[]{:S(2)}) collective-permute-start(bf16[1024,1024]{1,0:T(8,128)(2,1)} %bitcast.8), channel_id=1, source_target_pairs={{0,1},{1,0},{2,3},{3,2},{4,5},{5,4},{6,7},{7,6},{8,9},{9,8},{10,11... | collective-permute-start | bytes 6291464 | tf_op jit(solution)/shard_map/ppermute | solution.py:358
  1.4 0.1 collective-permute-start.8
  1.5 1.2 %shard_map.147 = bf16[16,1024]{1,0:T(8,128)(2,1)S(1)} custom-call(bf16[1024,1024]{1,0:T(8,128)(2,1)} %bitcast.9), custom_call_target="tpu_custom_call" | custom-call | flops 2147483648 | bytes 2097152 | tf_op jit(solution)/shard_map/pallas_call | solution.py:37
  2.6 3.5 %collective-permute-start.2 = (bf16[16,1024]{1,0:T(8,128)(2,1)S(1)}, bf16[16,1024]{1,0:T(8,128)(2,1)S(1)}, u32[]{:S(2)}, u32[]{:S(2)}) collective-permute-start(bf16[16,1024]{1,0:T(8,128)(2,1)S(1)} %shard_map.147), channel_id=1, source_target_pairs={{0,8},{8,16},{16,24},{24,32},{32,40},{40,48},{48,56},{56,64},{64,7... | collective-permute-start | bytes 98312 | tf_op jit(solution)/shard_map/ppermute | solution.py:359
  6.1 0.8 %collective-permute-start.10 = (bf16[512,2048]{1,0:T(8,128)(2,1)S(1)}, bf16[512,2048]{1,0:T(8,128)(2,1)S(1)}, u32[]{:S(2)}, u32[]{:S(2)}) collective-permute-start(bf16[512,2048]{1,0:T(8,128)(2,1)S(1)} %copy-done.2), channel_id=1, source_target_pairs={{0,1},{1,0},{2,3},{3,2},{4,5},{5,4},{6,7},{7,6},{8,9},{9,8},{10,11... | collective-permute-start | bytes 6291464 | tf_op jit(solution)/shard_map/ppermute | solution.py:469
  6.9 1.2 %shard_map.145.part = f32[1024,512]{1,0:T(8,128)S(1)} custom-call(bf16[1024,1024]{1,0:T(8,128)(2,1)S(1)} %bitcast.10, bf16[2048,512]{1,0:T(8,128)(2,1)S(1)} %copy-done.1), custom_call_target="tpu_custom_call" | custom-call | flops 1073741824 | bytes 4194304 | tf_op jit(solution)/shard_map/pallas_call | solution.py:37
  8.2 0.0 collective-permute-done.2.to
  8.2 0.2 collective-permute-start.3
  8.4 0.0 collective-permute-done.xp
  8.4 0.0 copy-start.12
  8.4 0.0 copy-start.13
  8.4 0.0 copy-start.14
  8.5 5.0 %shard_map.146 = (bf16[1024,512]{1,0:T(8,128)(2,1)S(1)}, bf16[1024,512]{1,0:T(8,128)(2,1)S(1)}, f32[1024,512]{1,0:T(8,128)S(1)}, bf16[4096,128]{1,0:T(8,128)(2,1...) custom-call(f32[1024,512]{1,0:T(8,128)S(1)} %shard_map.145.part, ...), custom_call_target="tpu_custom_call" | custom-call | flops 2147483648 | bytes 10504192 | tf_op jit(solution)/shard_map/pallas_call | solution.py:37
  13.5 0.0 collective-permute-done.3.tp
  13.5 0.0 copy-start.4
  13.5 3.3 %shard_map.148.po = bf16[1024,512]{1,0:T(8,128)(2,1)S(1)} custom-call(bf16[1024,1024]{1,0:T(8,128)(2,1)S(1)} %bitcast.12, bf16[1024,1024]{1,0:T(8,128)(2,1)S(1)} %collective-permute-done.xp, bf16[16,1024]{1,0:T(8,128)(2,1)S(1)} %collective-permute-done.2.to, bf16[16,1024]{1,0:T(8,128)(2,1)S(1)} %collective-permute-done.3.tp, ...), custom_call_target="tpu_custom_call" | custom-call | flops 2147483648 | bytes 6621184 | tf_op jit(solution)/shard_map/pallas_call | solution.py:37
  16.8 0.5 collective-permute-start.7
  17.3 1.7 %collective-permute-start.1 = (bf16[528,128]{1,0:T(8,128)(2,1)S(1)}, bf16[528,128]{1,0:T(8,128)(2,1)S(1)}, u32[]{:S(2)}, u32[]{:S(2)}) collective-permute-start(bf16[528,128]{1,0:T(8,128)(2,1)S(1)} %get-tuple-element.40), channel_id=1, source_target_pairs={{0,8},{8,0},{16,24},{24,16},{1,9},{9,1},{17,25},{25,17},{2,10},{10... | collective-permute-start | bytes 405512 | tf_op jit(solution)/shard_map/ppermute | solution.py:420
  19.0 3.5 %collective-permute-done.1.refs_0_ = bf16[528,128]{1,0:T(8,128)(2,1)S(1)} collective-permute-done((bf16[528,128]{1,0:T(8,128)(2,1)S(1)}, bf16[528,128]{1,0:T(8,128)(2,1)S(1)}, u32[]{:S(2)}, u32[]{:S(2)}) %collective-permute-start.1) | collective-permute-done | bytes 135200 | tf_op jit(solution)/shard_map/ppermute | solution.py:420
  22.6 0.1 shard_map.149
  22.7 2.5 %collective-permute-start.4 = (bf16[528,128]{1,0:T(8,128)(2,1)S(1)}, bf16[528,128]{1,0:T(8,128)(2,1)S(1)}, u32[]{:S(2)}, u32[]{:S(2)}) collective-permute-start(bf16[528,128]{1,0:T(8,128)(2,1)S(1)} %get-tuple-element.45), channel_id=1, source_target_pairs={{0,24},{24,0},{8,16},{16,8},{1,25},{25,1},{9,17},{17,9},{2,26},{26... | collective-permute-start | bytes 405512 | tf_op jit(solution)/shard_map/ppermute | solution.py:439
  25.2 3.3 %shard_map.150 = (bf16[1024,512]{1,0:T(8,128)(2,1)S(1)}, bf16[1024,512]{1,0:T(8,128)(2,1)S(1)}) custom-call(bf16[1024,1024]{1,0:T(8,128)(2,1)S(1)} %bitcast.13, bf16[1024,1024]{1,0:T(8,128)(2,1)S(1)} %collective-permute-done.xp, bf16[2048,512]{1,0:T(8,128)(2,1)S(1)} %copy-done.4, f32[1024,512]{1,0:T(8,128)S(1)} %get-tuple-element.47.rel, ...), custom_call_target="tpu_custom_call" | custom-call | flops 2147483648 | bytes 9437184 | tf_op jit(solution)/shard_map/pallas_call | solution.py:37
  28.6 0.0 collective-permute-done.4.refs_1_
  28.6 0.1 shard_map.151
  28.7 3.2 %collective-permute-start.5 = (bf16[528,128]{1,0:T(8,128)(2,1)S(1)}, bf16[528,128]{1,0:T(8,128)(2,1)S(1)}, u32[]{:S(2)}, u32[]{:S(2)}) collective-permute-start(bf16[528,128]{1,0:T(8,128)(2,1)S(1)} %get-tuple-element.53), channel_id=1, source_target_pairs={{0,32},{32,0},{64,96},{96,64},{1,33},{33,1},{65,97},{97,65},{2,34}... | collective-permute-start | bytes 405512 | tf_op jit(solution)/shard_map/ppermute | solution.py:453
  31.9 2.5 %shard_map.152.gate = f32[1024,512]{1,0:T(8,128)S(1)} custom-call(bf16[1024,1024]{1,0:T(8,128)(2,1)S(1)} %bitcast.14, bf16[1024,1024]{1,0:T(8,128)(2,1)S(1)} %collective-permute-done.xp, bf16[2048,512]{1,0:T(8,128)(2,1)S(1)} %copy-done.5, f32[1,128]{1,0:T(1,128)S(1)} %bitcast.22), custom_call_target="tpu_custom_call" | custom-call | flops 2147483648 | bytes 6291968 | tf_op jit(solution)/shard_map/pallas_call | solution.py:37
  34.5 0.0 collective-permute-done.5.refs_1_
  34.5 0.1 shard_map.153
  34.6 3.5 %collective-permute-start.6 = (bf16[528,128]{1,0:T(8,128)(2,1)S(1)}, bf16[528,128]{1,0:T(8,128)(2,1)S(1)}, u32[]{:S(2)}, u32[]{:S(2)}) collective-permute-start(bf16[528,128]{1,0:T(8,128)(2,1)S(1)} %get-tuple-element.56), channel_id=1, source_target_pairs={{0,96},{96,0},{32,64},{64,32},{1,97},{97,1},{33,65},{65,33},{2,98}... | collective-permute-start | bytes 405512 | tf_op jit(solution)/shard_map/ppermute | solution.py:467
  38.1 0.0 collective-permute-done.8.wp
  38.1 0.0 collective-permute-done.7.pp
  38.1 2.3 %shard_map.154.base = f32[1024,1024]{1,0:T(8,128)S(1)} custom-call(bf16[1024,1024]{1,0:T(8,128)(2,1)S(1)} %bitcast.15, bf16[1024,512]{1,0:T(8,128)(2,1)S(1)} %shard_map.148.po, bf16[1024,512]{1,0:T(8,128)(2,1)S(1)} %collective-permute-done.7.pp, bf16[512,2048]{1,0:T(8,128)(2,1)S(1)} %copy-done.6, bf16[512,2048]{1,0:T(8,128)(2,1)S(1)} %collective-permute-done.8.wp), custom_call_target="tpu_custom_call" | custom-call | flops 2147483648 | bytes 8388608 | tf_op jit(solution)/shard_map/pallas_call | solution.py:37
  40.4 0.0 collective-permute-done.6.recv
  40.5 0.9 %shard_map.157.ro = bf16[512,512]{1,0:T(8,128)(2,1)S(1)} custom-call(bf16[1024,512]{1,0:T(8,128)(2,1)S(1)} %get-tuple-element.60.scores, bf16[1024,512]{1,0:T(8,128)(2,1)S(1)} %get-tuple-element.61.up, bf16[1024,512]{1,0:T(8,128)(2,1)S(1)} %get-tuple-element.62.v, f32[1024,512]{1,0:T(8,128)S(1)} %shard_map.152.gate, ...), custom_call_target="tpu_custom_call" | custom-call | flops 536870912 | bytes 6709248 | tf_op jit(solution)/shard_map/pallas_call | solution.py:37
  41.3 4.5 %collective-permute-start.12 = (bf16[512,512]{1,0:T(8,128)(2,1)S(1)}, bf16[512,512]{1,0:T(8,128)(2,1)S(1)}, u32[]{:S(2)}, u32[]{:S(2)}) collective-permute-start(bf16[512,512]{1,0:T(8,128)(2,1)S(1)} %shard_map.157.ro), channel_id=1, source_target_pairs={{0,1},{1,0},{2,3},{3,2},{4,5},{5,4},{6,7},{7,6},{8,9},{9,8},{10,11... | collective-permute-start | bytes 1572872 | tf_op jit(solution)/shard_map/ppermute | solution.py:516
  45.9 0.8 %shard_map.155.ro = bf16[512,512]{1,0:T(8,128)(2,1)S(1)} custom-call(bf16[1024,512]{1,0:T(8,128)(2,1)S(1)} %get-tuple-element.60.scores, bf16[1024,512]{1,0:T(8,128)(2,1)S(1)} %get-tuple-element.61.up, bf16[1024,512]{1,0:T(8,128)(2,1)S(1)} %get-tuple-element.62.v, f32[1024,512]{1,0:T(8,128)S(1)} %shard_map.152.gate, ...), custom_call_target="tpu_custom_call" | custom-call | flops 536870912 | bytes 6709248 | tf_op jit(solution)/shard_map/pallas_call | solution.py:37
  46.7 0.1 collective-permute-start.9
  46.8 0.6 %collective-permute-done.12.rp = bf16[512,512]{1,0:T(8,128)(2,1)S(1)} collective-permute-done((bf16[512,512]{1,0:T(8,128)(2,1)S(1)}, bf16[512,512]{1,0:T(8,128)(2,1)S(1)}, u32[]{:S(2)}, u32[]{:S(2)}) %collective-permute-start.12) | collective-permute-done | bytes 524320 | tf_op jit(solution)/shard_map/ppermute | solution.py:516
  47.4 1.6 %shard_map.158 = (f32[512,1024]{1,0:T(8,128)S(1)}, f32[512,128]{1,0:T(8,128)S(1)}) custom-call(f32[1024,1024]{1,0:T(8,128)S(1)} %shard_map.154.base, bf16[512,512]{1,0:T(8,128)(2,1)S(1)} %shard_map.157.ro, bf16[512,512]{1,0:T(8,128)(2,1)S(1)} %collective-permute-done.12.rp, bf16[512,2048]{1,0:T(8,128)(2,1)S(1)} %copy-done.2, ...), custom_call_target="tpu_custom_call" | custom-call | flops 1073741824 | bytes 9437184 | tf_op jit(solution)/shard_map/pallas_call | solution.py:37
  49.0 0.0 copy-start.9
  49.0 0.5 collective-permute-start.13
  49.4 0.0 collective-permute-done.9.rp
  49.4 1.6 %shard_map.156 = (f32[512,1024]{1,0:T(8,128)S(1)}, f32[512,128]{1,0:T(8,128)S(1)}) custom-call(f32[1024,1024]{1,0:T(8,128)S(1)} %shard_map.154.base, bf16[512,512]{1,0:T(8,128)(2,1)S(1)} %shard_map.155.ro, bf16[512,512]{1,0:T(8,128)(2,1)S(1)} %collective-permute-done.9.rp, bf16[512,2048]{1,0:T(8,128)(2,1)S(1)} %copy-done.2, ...), custom_call_target="tpu_custom_call" | custom-call | flops 1073741824 | bytes 9437184 | tf_op jit(solution)/shard_map/pallas_call | solution.py:37
  51.0 0.2 collective-permute-start.11
  51.2 0.0 collective-permute-done.13.other
  51.2 1.5 %shard_map.159.before = bf16[1024,1024]{1,0:T(8,128)(2,1)} custom-call(f32[512,1024]{1,0:T(8,128)S(1)} %get-tuple-element.71.resid, f32[512,128]{1,0:T(8,128)S(1)} %get-tuple-element.72.own, f32[512,128]{1,0:T(8,128)S(1)} %collective-permute-done.13.other, f32[1,1024]{1,0:T(1,128)S(1)} %bitcast.17, f32[1,1024]{1,0:T(1,128)S(1)} %bitcast.19), custom_call_target="tpu_custom_call" | custom-call | flops 536870912 | bytes 2629632 | tf_op jit(solution)/shard_map/pallas_call | solution.py:37
  52.7 0.0 collective-permute-done.11.other
  52.7 1.4 %shard_map.160 = bf16[1024,1024]{1,0:T(8,128)(2,1)} custom-call(f32[512,1024]{1,0:T(8,128)S(1)} %get-tuple-element.68.resid, f32[512,128]{1,0:T(8,128)S(1)} %get-tuple-element.69.own, f32[512,128]{1,0:T(8,128)S(1)} %collective-permute-done.11.other, f32[1,1024]{1,0:T(1,128)S(1)} %bitcast.18, f32[1,1024]{1,0:T(1,128)S(1)} %bitcast.20, ...), custom_call_target="tpu_custom_call", output_to_operand_aliasing={{}: (5, {})} | custom-call | flops 536870912 | bytes 4726784 | tf_op jit(solution)/shard_map/pallas_call | solution.py:37
  (26 shorter events, 0.1 us)
Async XLA Ops:
  0.0 6.1 %copy-start.2 = (bf16[512,2048]{1,0:T(8,128)(2,1)S(1)}, bf16[512,2048]{1,0:T(8,128)(2,1)}, u32[]{:S(2)}) copy-start(bf16[512,2048]{1,0:T(8,128)(2,1)} %wo.5) | copy-start | bytes 6291460
  0.0 6.9 %copy-start = (bf16[1,1024,1024]{2,1,0:T(8,128)(2,1)S(1)}, bf16[1,1024,1024]{2,1,0:T(8,128)(2,1)}, u32[]{:S(2)}) copy-start(bf16[1,1024,1024]{2,1,0:T(8,128)(2,1)} %param.15) | copy-start | bytes 6291460
  0.0 6.9 %copy-start.1 = (bf16[2048,512]{1,0:T(8,128)(2,1)S(1)}, bf16[2048,512]{1,0:T(8,128)(2,1)}, u32[]{:S(2)}) copy-start(bf16[2048,512]{1,0:T(8,128)(2,1)} %wf.3) | copy-start | bytes 6291460
  0.0 8.4 %collective-permute-start = (bf16[1024,1024]{1,0:T(8,128)(2,1)}, bf16[1024,1024]{1,0:T(8,128)(2,1)S(1)}, u32[]{:S(2)}, u32[]{:S(2)}) collective-permute-start(bf16[1024,1024]{1,0:T(8,128)(2,1)} %bitcast.8), channel_id=1, source_target_pairs={{0,1},{1,0},{2,3},{3,2},{4,5},{5,4},{6,7},{7,6},{8,9},{9,8},{10,11... | collective-permute-start | bytes 6291464 | tf_op jit(solution)/shard_map/ppermute | solution.py:358
  1.4 36.7 %collective-permute-start.8 = (bf16[512,2048]{1,0:T(8,128)(2,1)}, bf16[512,2048]{1,0:T(8,128)(2,1)S(1)}, u32[]{:S(2)}, u32[]{:S(2)}) collective-permute-start(bf16[512,2048]{1,0:T(8,128)(2,1)} %wo.3), channel_id=1, source_target_pairs={{0,1},{1,0},{2,3},{3,2},{4,5},{5,4},{6,7},{7,6},{8,9},{9,8},{10,11... | collective-permute-start | bytes 6291464 | tf_op jit(solution)/shard_map/ppermute | solution.py:468
  2.6 5.8 %copy-start.3 = (bf16[2048,512]{1,0:T(8,128)(2,1)S(1)}, bf16[2048,512]{1,0:T(8,128)(2,1)}, u32[]{:S(2)}) copy-start(bf16[2048,512]{1,0:T(8,128)(2,1)} %wv.1) | copy-start | bytes 6291460
  2.6 5.8 %copy-start.7 = (f32[1024,4]{0,1:T(4,128)S(1)}, f32[1024,4]{0,1:T(4,128)}, u32[]{:S(2)}) copy-start(f32[1024,4]{0,1:T(4,128)} %param.24) | copy-start | bytes 49156
  2.6 5.8 %copy-start.10 = (f32[512]{0:T(512)S(1)}, f32[512]{0:T(512)}, u32[]{:S(2)}) copy-start(f32[512]{0:T(512)} %param.23) | copy-start | bytes 6148
  2.6 5.5 %collective-permute-start.2 = (bf16[16,1024]{1,0:T(8,128)(2,1)S(1)}, bf16[16,1024]{1,0:T(8,128)(2,1)S(1)}, u32[]{:S(2)}, u32[]{:S(2)}) collective-permute-start(bf16[16,1024]{1,0:T(8,128)(2,1)S(1)} %shard_map.147), channel_id=1, source_target_pairs={{0,8},{8,16},{16,24},{24,32},{32,40},{40,48},{48,56},{56,64},{64,7... | collective-permute-start | bytes 98312 | tf_op jit(solution)/shard_map/ppermute | solution.py:359
  6.1 40.7 %collective-permute-start.10 = (bf16[512,2048]{1,0:T(8,128)(2,1)S(1)}, bf16[512,2048]{1,0:T(8,128)(2,1)S(1)}, u32[]{:S(2)}, u32[]{:S(2)}) collective-permute-start(bf16[512,2048]{1,0:T(8,128)(2,1)S(1)} %copy-done.2), channel_id=1, source_target_pairs={{0,1},{1,0},{2,3},{3,2},{4,5},{5,4},{6,7},{7,6},{8,9},{9,8},{10,11... | collective-permute-start | bytes 6291464 | tf_op jit(solution)/shard_map/ppermute | solution.py:469
  8.2 5.3 %collective-permute-start.3 = (bf16[16,1024]{1,0:T(8,128)(2,1)S(1)}, bf16[16,1024]{1,0:T(8,128)(2,1)S(1)}, u32[]{:S(2)}, u32[]{:S(2)}) collective-permute-start(bf16[16,1024]{1,0:T(8,128)(2,1)S(1)} %collective-permute-done.2.to), channel_id=1, source_target_pairs={{0,1},{1,0},{2,3},{3,2},{4,5},{5,4},{6,7},{7,6},{8,9},{9,8},{10,11... | collective-permute-start | bytes 98312 | tf_op jit(solution)/shard_map/ppermute | solution.py:360
  8.4 5.0 %copy-start.12 = (bf16[2048,512]{1,0:T(8,128)(2,1)S(1)}, bf16[2048,512]{1,0:T(8,128)(2,1)}, u32[]{:S(2)}) copy-start(bf16[2048,512]{1,0:T(8,128)(2,1)} %w.3) | copy-start | bytes 6291460
  8.4 5.0 %copy-start.13 = (bf16[2,256,256]{2,1,0:T(8,128)(2,1)S(1)}, bf16[2,256,256]{2,1,0:T(8,128)(2,1)}, u32[]{:S(2)}) copy-start(bf16[2,256,256]{2,1,0:T(8,128)(2,1)} %mix.1) | copy-start | bytes 786436
  8.4 5.0 %copy-start.14 = (f32[512]{0:T(512)S(1)}, f32[512]{0:T(512)}, u32[]{:S(2)}) copy-start(f32[512]{0:T(512)} %param.22) | copy-start | bytes 6148
  13.5 11.7 %copy-start.4 = (bf16[2048,512]{1,0:T(8,128)(2,1)S(1)}, bf16[2048,512]{1,0:T(8,128)(2,1)}, u32[]{:S(2)}) copy-start(bf16[2048,512]{1,0:T(8,128)(2,1)} %w.4) | copy-start | bytes 6291460
  16.8 21.2 %collective-permute-start.7 = (bf16[1024,512]{1,0:T(8,128)(2,1)S(1)}, bf16[1024,512]{1,0:T(8,128)(2,1)S(1)}, u32[]{:S(2)}, u32[]{:S(2)}) collective-permute-start(bf16[1024,512]{1,0:T(8,128)(2,1)S(1)} %shard_map.148.po), channel_id=1, source_target_pairs={{0,1},{1,0},{2,3},{3,2},{4,5},{5,4},{6,7},{7,6},{8,9},{9,8},{10,11... | collective-permute-start | bytes 3145736 | tf_op jit(solution)/shard_map/ppermute | solution.py:435
  17.3 5.3 %collective-permute-start.1 = (bf16[528,128]{1,0:T(8,128)(2,1)S(1)}, bf16[528,128]{1,0:T(8,128)(2,1)S(1)}, u32[]{:S(2)}, u32[]{:S(2)}) collective-permute-start(bf16[528,128]{1,0:T(8,128)(2,1)S(1)} %get-tuple-element.40), channel_id=1, source_target_pairs={{0,8},{8,0},{16,24},{24,16},{1,9},{9,1},{17,25},{25,17},{2,10},{10... | collective-permute-start | bytes 405512 | tf_op jit(solution)/shard_map/ppermute | solution.py:420
  22.7 5.9 %collective-permute-start.4 = (bf16[528,128]{1,0:T(8,128)(2,1)S(1)}, bf16[528,128]{1,0:T(8,128)(2,1)S(1)}, u32[]{:S(2)}, u32[]{:S(2)}) collective-permute-start(bf16[528,128]{1,0:T(8,128)(2,1)S(1)} %get-tuple-element.45), channel_id=1, source_target_pairs={{0,24},{24,0},{8,16},{16,8},{1,25},{25,1},{9,17},{17,9},{2,26},{26... | collective-permute-start | bytes 405512 | tf_op jit(solution)/shard_map/ppermute | solution.py:439
  25.2 6.7 %copy-start.5 = (bf16[2048,512]{1,0:T(8,128)(2,1)S(1)}, bf16[2048,512]{1,0:T(8,128)(2,1)}, u32[]{:S(2)}) copy-start(bf16[2048,512]{1,0:T(8,128)(2,1)} %w.5) | copy-start | bytes 6291460
  25.2 6.7 %copy-start.11 = (f32[128]{0:T(128)S(1)}, f32[128]{0:T(128)}, u32[]{:S(2)}) copy-start(f32[128]{0:T(128)} %param.25) | copy-start | bytes 1540
  28.7 5.8 %collective-permute-start.5 = (bf16[528,128]{1,0:T(8,128)(2,1)S(1)}, bf16[528,128]{1,0:T(8,128)(2,1)S(1)}, u32[]{:S(2)}, u32[]{:S(2)}) collective-permute-start(bf16[528,128]{1,0:T(8,128)(2,1)S(1)} %get-tuple-element.53), channel_id=1, source_target_pairs={{0,32},{32,0},{64,96},{96,64},{1,33},{33,1},{65,97},{97,65},{2,34}... | collective-permute-start | bytes 405512 | tf_op jit(solution)/shard_map/ppermute | solution.py:453
  31.9 6.2 %copy-start.6 = (bf16[512,2048]{1,0:T(8,128)(2,1)S(1)}, bf16[512,2048]{1,0:T(8,128)(2,1)}, u32[]{:S(2)}) copy-start(bf16[512,2048]{1,0:T(8,128)(2,1)} %wo.3) | copy-start | bytes 6291460
  34.6 5.9 %collective-permute-start.6 = (bf16[528,128]{1,0:T(8,128)(2,1)S(1)}, bf16[528,128]{1,0:T(8,128)(2,1)S(1)}, u32[]{:S(2)}, u32[]{:S(2)}) collective-permute-start(bf16[528,128]{1,0:T(8,128)(2,1)S(1)} %get-tuple-element.56), channel_id=1, source_target_pairs={{0,96},{96,0},{32,64},{64,32},{1,97},{97,1},{33,65},{65,33},{2,98}... | collective-permute-start | bytes 405512 | tf_op jit(solution)/shard_map/ppermute | solution.py:467
  41.3 6.1 %collective-permute-start.12 = (bf16[512,512]{1,0:T(8,128)(2,1)S(1)}, bf16[512,512]{1,0:T(8,128)(2,1)S(1)}, u32[]{:S(2)}, u32[]{:S(2)}) collective-permute-start(bf16[512,512]{1,0:T(8,128)(2,1)S(1)} %shard_map.157.ro), channel_id=1, source_target_pairs={{0,1},{1,0},{2,3},{3,2},{4,5},{5,4},{6,7},{7,6},{8,9},{9,8},{10,11... | collective-permute-start | bytes 1572872 | tf_op jit(solution)/shard_map/ppermute | solution.py:516
  46.7 2.7 %collective-permute-start.9 = (bf16[512,512]{1,0:T(8,128)(2,1)S(1)}, bf16[512,512]{1,0:T(8,128)(2,1)S(1)}, u32[]{:S(2)}, u32[]{:S(2)}) collective-permute-start(bf16[512,512]{1,0:T(8,128)(2,1)S(1)} %shard_map.155.ro), channel_id=1, source_target_pairs={{0,1},{1,0},{2,3},{3,2},{4,5},{5,4},{6,7},{7,6},{8,9},{9,8},{10,11... | collective-permute-start | bytes 1572872 | tf_op jit(solution)/shard_map/ppermute | solution.py:516
  49.0 2.3 %copy-start.8 = (f32[1024]{0:T(1024)S(1)}, f32[1024]{0:T(1024)}, u32[]{:S(2)}) copy-start(f32[1024]{0:T(1024)} %param.28) | copy-start | bytes 12292
  49.0 2.3 %copy-start.9 = (f32[1024]{0:T(1024)S(1)}, f32[1024]{0:T(1024)}, u32[]{:S(2)}) copy-start(f32[1024]{0:T(1024)} %param.29) | copy-start | bytes 12292
  49.0 2.2 %collective-permute-start.13 = (f32[512,128]{1,0:T(8,128)S(1)}, f32[512,128]{1,0:T(8,128)S(1)}, u32[]{:S(2)}, u32[]{:S(2)}) collective-permute-start(f32[512,128]{1,0:T(8,128)S(1)} %get-tuple-element.72.own), channel_id=1, source_target_pairs={{0,1},{1,0},{2,3},{3,2},{4,5},{5,4},{6,7},{7,6},{8,9},{9,8},{10,11... | collective-permute-start | bytes 786440 | tf_op jit(solution)/shard_map/ppermute | solution.py:533
  51.0 1.7 %collective-permute-start.11 = (f32[512,128]{1,0:T(8,128)S(1)}, f32[512,128]{1,0:T(8,128)S(1)}, u32[]{:S(2)}, u32[]{:S(2)}) collective-permute-start(f32[512,128]{1,0:T(8,128)S(1)} %get-tuple-element.69.own), channel_id=1, source_target_pairs={{0,1},{1,0},{2,3},{3,2},{4,5},{5,4},{6,7},{7,6},{8,9},{9,8},{10,11... | collective-permute-start | bytes 786440 | tf_op jit(solution)/shard_map/ppermute | solution.py:543
